TPU v7x, 32 devices: a whole 2x2x4 slice. The times are simulated.
32 devices in a mesh: sp: 8 (over z, x), dp: 4 (over y, core).
Axes of the slice: x: 2, y: 2, z: 4, core: 2. Of those that a mesh axis runs over, the one named last changes fastest.
Arguments:
- queries: bfloat16 [16, 8, 512, 128], P('dp', None, 'sp'), may hold values from -6 to 6
- keys: bfloat16 [16, 8, 512, 128], P('dp', None, 'sp'), may hold values from -6 to 6
- values: bfloat16 [16, 8, 512, 128], P('dp', None, 'sp'), may hold values from -6 to 6
- input_gate: bfloat16 [16, 8, 512], P('dp', None, 'sp'), may hold values from -6 to 140
- forget_gate: bfloat16 [16, 8, 512], P('dp', None, 'sp'), may hold values from 0.5 to 11.5
- start_memory: float32 [16, 8, 128, 128], P('dp', None, 'sp'), may hold values from -6 to 6
- start_norm: float32 [16, 8, 128], P('dp', None, 'sp'), may hold values from -24 to 24
- start_level: float32 [16, 8], P('dp'), may hold values from 2 to 4
- head_gain: float32 [8, 128], replicated, may hold values from 0.1 to 1.9
- out_weight: bfloat16 [1024, 4096], P(None, 'dp'), may hold values from -0.1875 to 0.1875
Outputs:
- mixed: bfloat16 [16, 512, 4096], P('dp', 'sp')
All inputs are finite; a program needn't handle non-finite values.
Results may differ from a plain program's by a relative error of at most 0.019.
Values may be sent and summed in bfloat16 or wider, within the bound.
A program may use at most 64 MiB of HBM per device.

v0:
```python
import jax
import jax.numpy as jnp
from jax import lax
from jax.experimental import pallas as pl
from jax.experimental.pallas import tpu as pltpu
from jax.sharding import PartitionSpec as P

ROWS = 256
SUB = 8
FILL = -1e30


def cell_kernel(count, tokens, x_ref, mem_ref, in_ref, keep_ref, norm_ref, level_ref, o_ref):
    group = x_ref.shape[0]
    width = x_ref.shape[3]
    length = group * tokens
    factor = width ** (-0.5)
    lane = lax.broadcasted_iota(jnp.int32, in_ref.shape, 1)
    total = keep_ref[...]
    step = 1
    while step < length:
        total = total + jnp.where(lane >= step, pltpu.roll(total, step, 1), 0.0)
        step *= 2
    offset = in_ref[...] - total
    peak = offset
    step = 1
    while step < length:
        peak = jnp.maximum(peak, jnp.where(lane >= step, pltpu.roll(peak, step, 1), FILL))
        step *= 2
    level = level_ref[...]
    peak = jnp.maximum(peak, level)
    carry = jnp.transpose(jnp.exp(level - peak))
    peak = jnp.transpose(peak)
    rows = tokens
    while rows * 2 <= ROWS and length % (rows * 2) == 0:
        rows *= 2
    for i in range(count):
        query = x_ref[:, i, 0:tokens, :].reshape(length, width)
        key = x_ref[:, i, tokens : 2 * tokens, :].reshape(length, width)
        value = x_ref[:, i, 2 * tokens : 3 * tokens, :].reshape(length, width)
        memory = mem_ref[i]
        norm = norm_ref[i : i + 1, :]
        for first in range(0, length, rows):
            end = first + rows
            part = query[first:end]
            raw = lax.dot_general(
                part, key[:end], (((1,), (1,)), ((), ())), preferred_element_type=jnp.float32
            )
            here = first + lax.broadcasted_iota(jnp.int32, (rows, end), 0)
            there = lax.broadcasted_iota(jnp.int32, (rows, end), 1)
            gap = offset[i : i + 1, :end] - peak[first:end, i : i + 1]
            decay = jnp.exp(jnp.where(there <= here, gap, FILL))
            scores = raw * factor * decay
            weight = carry[first:end, i : i + 1] * factor
            num = jnp.dot(
                scores.astype(jnp.bfloat16), value[:end], preferred_element_type=jnp.float32
            ) + weight * jnp.dot(part, memory, preferred_element_type=jnp.float32)
            den = jnp.sum(scores, axis=1, keepdims=True) + weight * jnp.sum(
                part.astype(jnp.float32) * norm, axis=1, keepdims=True
            )
            out = (num / jnp.maximum(jnp.abs(den), 1.0)).astype(o_ref.dtype)
            for piece in range(rows // tokens):
                o_ref[first // tokens + piece, i] = out[piece * tokens : (piece + 1) * tokens]


def on_device(
    queries,
    keys,
    values,
    input_gate,
    forget_gate,
    start_memory,
    start_norm,
    start_level,
    head_gain,
    out_weight,
):
    seqs, heads, tokens, width = queries.shape
    count = seqs * heads
    group = lax.axis_size("sp")
    owned = count // group
    length = group * tokens
    channels = start_memory.shape[2]

    def items(tensor):
        return tensor.reshape((group, owned) + tensor.shape[2:])

    small = jnp.concatenate(
        [items(input_gate), items(forget_gate), items(start_norm).astype(jnp.bfloat16)], axis=2
    )
    lines = -(-small.shape[2] // (16 * width)) * 16
    small = jnp.pad(small, ((0, 0), (0, 0), (0, lines * width - small.shape[2])))
    packed = jnp.concatenate(
        [
            items(queries),
            items(keys),
            items(values),
            items(start_memory).astype(jnp.bfloat16),
            small.reshape(group, owned, lines, width),
        ],
        axis=2,
    )
    got = lax.all_to_all(packed, "sp", split_axis=0, concat_axis=0, tiled=True)
    base = 3 * tokens
    memory = jnp.moveaxis(got[:, :, base : base + channels], 0, 1).reshape(owned, width, width)
    tail = jnp.moveaxis(got[:, :, base + channels :], 0, 1).reshape(owned, group, lines * width)
    tail = tail.astype(jnp.float32)
    extra = (-owned) % SUB

    def padded(tensor):
        return jnp.pad(tensor.reshape(owned, -1), ((0, extra), (0, 0)))

    gate_in = padded(tail[:, :, :tokens])
    gate_keep = padded(jax.nn.log_sigmoid(tail[:, :, tokens : 2 * tokens]))
    norm = padded(tail[:, :, 2 * tokens : 2 * tokens + channels])
    level = padded(
        lax.dynamic_slice_in_dim(start_level.reshape(count), lax.axis_index("sp") * owned, owned)
    )
    hidden = pl.pallas_call(
        lambda *refs: cell_kernel(owned, tokens, *refs),
        out_shape=jax.ShapeDtypeStruct((group, owned, tokens, width), jnp.bfloat16),
        in_specs=[pl.BlockSpec(memory_space=pltpu.VMEM)] * 6,
        out_specs=pl.BlockSpec(memory_space=pltpu.VMEM),
        cost_estimate=pl.CostEstimate(
            flops=4 * owned * length * length * width,
            bytes_accessed=2 * got.size,
            transcendentals=owned * length * length,
        ),
        compiler_params=pltpu.CompilerParams(vmem_limit_bytes=48 * 1024 * 1024),
        name="cell",
    )(got, memory, gate_in, gate_keep, norm, level)
    returned = lax.all_to_all(hidden, "sp", split_axis=0, concat_axis=0, tiled=True)
    returned = returned.reshape(seqs, heads, tokens, width)
    normed = (returned.astype(jnp.float32) * head_gain[:, None, :]).astype(jnp.bfloat16)
    flat = jnp.moveaxis(normed, 1, 2).reshape(seqs * tokens, heads * width)
    weight = lax.all_gather(out_weight, "dp", axis=1, tiled=True)
    mixed = jnp.dot(flat, weight, preferred_element_type=jnp.float32).astype(jnp.bfloat16)
    return mixed.reshape(seqs, tokens, weight.shape[1])


def solution(mesh):
    in_specs = (
        P("dp", None, "sp", None),
        P("dp", None, "sp", None),
        P("dp", None, "sp", None),
        P("dp", None, "sp"),
        P("dp", None, "sp"),
        P("dp", None, "sp", None),
        P("dp", None, "sp"),
        P("dp", None),
        P(),
        P(None, "dp"),
    )
    out_specs = P("dp", "sp", None)
    return jax.shard_map(
        on_device, mesh=mesh, in_specs=in_specs, out_specs=out_specs, check_vma=False
    )
```

profile of v0, /device:TPU:0, one launch (start us, length us, event | category | flops | bytes accessed | tf_op | source)
XLA Modules:
  0.0 98.7 jit_solution(10069744556744076313)
XLA Ops:
  6.5 0.0 copy-start.3
  6.5 0.0 copy-start.4
  6.5 0.0 copy-start.6
  6.5 0.0 copy-start.5
  6.5 0.0 copy-start
  6.5 0.0 copy-start.1
  6.6 0.0 all-gather.2.cloned.1.call-start
  6.6 0.7 all-gather.2.cloned.1.call-update
  7.3 0.2 copy-done.3
  7.5 0.0 copy-start.2
  7.5 0.0 copy-done.4
  7.5 0.0 copy-done.6
  7.5 0.0 copy-done.5
  7.6 0.1 fusion.7
  7.6 0.1 reshape.58
  7.7 0.0 copy-done
  7.7 0.9 constant_dynamic-update-slice_fusion.4
  8.7 0.0 copy-done.1
  8.7 0.9 constant_dynamic-update-slice_fusion.3
  9.6 0.0 copy-done.2
  9.6 0.9 constant_dynamic-update-slice_fusion.2
  10.6 0.7 constant_dynamic-update-slice_fusion.1
  11.2 0.7 constant_dynamic-update-slice_fusion
  11.9 0.0 copy-start.8
  11.9 7.4 %all-to-all-start = ((bf16[8,4,224,128]{3,2,1,0:T(8,128)(2,1)}), bf16[8,4,224,128]{3,2,1,0:T(8,128)(2,1)S(1)}, u32[]{:S(2)}, u32[]{:S(2)}) async-start(bf16[8,4,224,128]{3,2,1,0:T(8,128)(2,1)} %constant_dynamic-update-slice_fusion), calls=%async_computation | async-start | bytes 3670016 | tf_op jit(solution)/shard_map/all_to_all | solution.py:103
  19.3 0.0 copy-done.8
  19.3 0.1 reshape.63
  19.4 0.1 dynamic-slice_bitcast_fusion
  19.5 0.1 copy.20
  19.6 42.3 %all-to-all-done.refs_0_ = bf16[8,4,224,128]{3,2,1,0:T(8,128)(2,1)S(1)} async-done(((bf16[8,4,224,128]{3,2,1,0:T(8,128)(2,1)}), bf16[8,4,224,128]{3,2,1,0:T(8,128)(2,1)S(1)}, u32[]{:S(2)}, u32[]{:S(2)}) %all-to-all-start) | async-done | bytes 1835040 | tf_op jit(solution)/shard_map/all_to_all | solution.py:103
  62.0 0.1 reshape.67
  62.1 0.1 fusion.9
  62.2 0.1 reshape.60
  62.3 0.1 reshape.61
  62.4 0.1 reshape.62
  62.5 3.4 %cell.1 = bf16[8,4,64,128]{3,2,1,0:T(8,128)(2,1)S(1)} custom-call(bf16[8,4,224,128]{3,2,1,0:T(8,128)(2,1)S(1)} %all-to-all-done.refs_0_, bf16[4,128,128]{2,1,0:T(8,128)(2,1)S(1)} %bitcast.30, f32[8,512]{1,0:T(8,128)S(1)} %pad.20.refs_2_, f32[8,512]{1,0:T(8,128)S(1)} %pad.21.refs_3_, f32[8,128]{1,0:T(8,128)S(1)} %pad.22.refs_4_, f32[8,1]{1,0:T(8,128)S(1)} %pad.23.refs_5_), custom_call_target="tpu_custom_call" | custom-call | flops 536870912 | bytes 1835008 | tf_op jit(solution)/shard_map/cell/pallas_call | solution.py:119
  65.9 0.0 copy-start.7
  65.9 18.1 %all_to_all.10 = bf16[8,4,64,128]{3,2,1,0:T(8,128)(2,1)S(1)} all-to-all(bf16[8,4,64,128]{3,2,1,0:T(8,128)(2,1)S(1)} %cell.1), channel_id=1, replica_groups=mesh['sp'=8,'dp'=4] {'sp'}, dimensions={0} | all-to-all | bytes 1048576 | tf_op jit(solution)/shard_map/all_to_all | solution.py:132
  84.0 0.1 bitcast_convert_fusion
  84.2 0.0 copy-done.7
  84.2 0.6 fusion
  84.8 0.0 all-gather.2.cloned.1.call-done
  84.8 7.0 %convolution_convert_fusion = bf16[256,4096]{1,0:T(8,128)(2,1)} fusion(bf16[1024,4096]{1,0:T(8,128)(2,1)} %all-gather.2.cloned.1.call-done, bf16[32,8,8,128]{3,2,1,0:T(8,128)(2,1)S(1)} %bitcast.32), kind=kOutput, calls=%fused_computation | convolution fusion | flops 2148532224 | bytes 11010048 | tf_op jit(solution)/shard_map/dot_general | solution.py:137
  (12 shorter events, 0.1 us)
Async XLA Ops:
  6.5 0.9 copy-start.3
  6.5 1.0 copy-start.4
  6.5 1.0 %copy-start.6 = (bf16[4,8,64]{2,1,0:T(8,128)(2,1)S(1)}, bf16[4,8,64]{2,1,0:T(8,128)(2,1)}, u32[]{:S(2)}) copy-start(bf16[4,8,64]{2,1,0:T(8,128)(2,1)} %param.13) | copy-start | bytes 12292
  6.5 1.0 %copy-start.5 = (bf16[4,8,64]{2,1,0:T(8,128)(2,1)S(1)}, bf16[4,8,64]{2,1,0:T(8,128)(2,1)}, u32[]{:S(2)}) copy-start(bf16[4,8,64]{2,1,0:T(8,128)(2,1)} %param.14) | copy-start | bytes 12292
  6.5 1.2 %copy-start = (bf16[4,8,64,128]{3,2,1,0:T(8,128)(2,1)S(1)}, bf16[4,8,64,128]{3,2,1,0:T(8,128)(2,1)}, u32[]{:S(2)}) copy-start(bf16[4,8,64,128]{3,2,1,0:T(8,128)(2,1)} %param.10) | copy-start | bytes 1572868
  6.5 2.1 %copy-start.1 = (bf16[4,8,64,128]{3,2,1,0:T(8,128)(2,1)S(1)}, bf16[4,8,64,128]{3,2,1,0:T(8,128)(2,1)}, u32[]{:S(2)}) copy-start(bf16[4,8,64,128]{3,2,1,0:T(8,128)(2,1)} %param.11) | copy-start | bytes 1572868
  6.6 78.3 %all-gather.2.cloned.1.call-start = ((), (), s32[]{:S(2)}) async-start(), calls=%async_computation.2 | async-start | bytes 10485760 | tf_op jit(solution)/shard_map/all_gather | solution.py:136
  7.5 2.1 %copy-start.2 = (bf16[4,8,64,128]{3,2,1,0:T(8,128)(2,1)S(1)}, bf16[4,8,64,128]{3,2,1,0:T(8,128)(2,1)}, u32[]{:S(2)}) copy-start(bf16[4,8,64,128]{3,2,1,0:T(8,128)(2,1)} %param.12) | copy-start | bytes 1572868
  11.9 7.4 %copy-start.8 = (f32[4,8]{1,0:T(4,128)S(1)}, f32[4,8]{1,0:T(4,128)}, u32[]{:S(2)}) copy-start(f32[4,8]{1,0:T(4,128)} %param.17) | copy-start | bytes 388
  11.9 50.0 %all-to-all-start = ((bf16[8,4,224,128]{3,2,1,0:T(8,128)(2,1)}), bf16[8,4,224,128]{3,2,1,0:T(8,128)(2,1)S(1)}, u32[]{:S(2)}, u32[]{:S(2)}) async-start(bf16[8,4,224,128]{3,2,1,0:T(8,128)(2,1)} %constant_dynamic-update-slice_fusion), calls=%async_computation | async-start | bytes 3670016 | tf_op jit(solution)/shard_map/all_to_all | solution.py:103
  65.9 18.2 %copy-start.7 = (f32[8,128]{1,0:T(8,128)S(1)}, f32[8,128]{1,0:T(8,128)}, u32[]{:S(2)}) copy-start(f32[8,128]{1,0:T(8,128)} %param.18) | copy-start | bytes 12292
Sparse Core Ops, SparseCore 0:
  8.9 60.9 all-gather.1
where the time goes:
time: 99 us; the launch traced here: 98.7 us
  waiting for transfers between devices  43.1 us (44%)
  blocking collectives  18.1 us (18%)
  between operations  13.6 us (14%)
  starting transfers between devices  7.45 us (8%)
  matrix products  7.04 us (7%)
  local copies, waits for them, and re-layouts  5.18 us (5%)
  Pallas kernels  3.43 us (3%)
    all_to_all x1, waiting for transfers between devices, on_device(): got = lax.all_to_all(packed, 'sp', split_axis=0, concat_axis=0, tiled=True)  42.3 us
    all_to_all x1, blocking collectives, on_device(): lax.all_to_all(hidden, 'sp', split_axis=0, concat_axis=0, tiled=True)  18.1 us
    all_to_all x1, starting transfers between devices, on_device(): got = lax.all_to_all(packed, 'sp', split_axis=0, concat_axis=0, tiled=True)  7.41 us
    dot_general x1, matrix products, on_device(): jnp.dot(flat, weight, preferred_element_type=jnp.float32)  7.04 us
    unnamed x24, local copies, waits for them, and re-layouts  3.71 us
    pallas_call x1, Pallas kernels, on_device(): pl.pallas_call(lambda *refs: cell_kernel(owned, tokens, *refs), out_shape...  3.43 us
  transfers between devices with their start and end apart: 2, of which 1 were waited for; matrix products, arithmetic and copies ran while one was open for 6% of the time, Pallas kernels for 3%

commit v1 on v0

v1 whole, which is shorter than its diff:
```python
import jax
import jax.numpy as jnp
from jax import lax
from jax.experimental import pallas as pl
from jax.experimental.pallas import tpu as pltpu
from jax.sharding import PartitionSpec as P

MESH = pl.DeviceIdType.MESH
FILL = -1e30
PER = 2
HOP = 3
PIECES = 16
SKIP = 7
TAIL = 16


def layer_kernel(
    sizes,
    q_hbm,
    k_hbm,
    v_hbm,
    ig_hbm,
    fg_hbm,
    w_hbm,
    mem_ref,
    norm_ref,
    level_ref,
    gain_ref,
    out_ref,
    xq,
    xk,
    xv,
    igr,
    fgr,
    cast,
    mem_in,
    norm_in,
    norm_out,
    offs,
    peaks,
    starts,
    off_g,
    wrow,
    arow,
    srow,
    pcol,
    grown,
    st_in,
    st_out,
    act,
    back,
    weight,
    loc_sem,
    gate_send,
    gate_recv,
    x_send,
    x_recv,
    mem_send,
    mem_recv,
    st_send,
    st_recv,
    back_send,
    back_recv,
    wy_send,
    wy_recv,
    wz_send,
    wz_recv,
    wd_send,
    wd_recv,
    own_send,
    own_recv,
):
    n_sp, n_dp, seqs, heads, tokens, width, channels = sizes
    n_groups = n_sp // 2
    chips = n_dp // 2
    half = seqs // 2
    items = half * heads
    span = 2 * tokens
    chunks = items // PER
    per_seq = heads // PER
    rows = w_hbm.shape[0] // PIECES
    factor = width ** (-0.5)
    f32, bf16 = jnp.float32, jnp.bfloat16

    sp, dp = lax.axis_index("sp"), lax.axis_index("dp")
    g, m = sp // 2, sp % 2
    y, core = dp // 2, dp % 2
    mate = g * 2 + (1 - m)
    twin = y * 2 + (1 - core)
    even = 1 - g % 2

    def remote(src, dst, send, recv, to_sp, to_dp):
        return pltpu.make_async_remote_copy(
            src_ref=src,
            dst_ref=dst,
            send_sem=send,
            recv_sem=recv,
            device_id=(to_sp, to_dp),
            device_id_type=MESH,
        )

    mine = pl.ds(half * m, half)
    here = pl.ds(pl.multiple_of(m * tokens, tokens), tokens)
    local = [
        pltpu.make_async_copy(ig_hbm.at[mine], igr.at[sp], loc_sem.at[0]),
        pltpu.make_async_copy(fg_hbm.at[mine], fgr.at[sp], loc_sem.at[1]),
        pltpu.make_async_copy(k_hbm.at[mine], xk.at[:, :, here, :], loc_sem.at[2]),
        pltpu.make_async_copy(v_hbm.at[mine], xv.at[:, :, here, :], loc_sem.at[3]),
        pltpu.make_async_copy(q_hbm.at[mine], xq.at[:, :, here, :], loc_sem.at[4]),
        pltpu.make_async_copy(w_hbm, weight.at[dp], loc_sem.at[5]),
    ]
    for copy in local:
        copy.start()

    barrier = pltpu.get_barrier_semaphore()
    for d in range(1, n_sp):
        pl.semaphore_signal(barrier, inc=1, device_id=((sp + d) % n_sp, dp), device_id_type=MESH)
    pl.semaphore_signal(barrier, inc=1, device_id=(sp, twin), device_id_type=MESH)
    for j in range(1, chips):
        pl.semaphore_signal(
            barrier, inc=1, device_id=(sp, ((y + j) % chips) * 2 + core), device_id_type=MESH
        )
    cast[...] = mem_ref[...].astype(bf16)
    pl.semaphore_wait(barrier, n_sp - 1 + 1 + chips - 1)

    def gate_copy(d):
        to = (sp + d) % n_sp
        part = pl.ds(half * (to % 2), half)
        return [
            remote(ig_hbm.at[part], igr.at[sp], gate_send.at[0, d], gate_recv.at[0, d], to, dp),
            remote(fg_hbm.at[part], fgr.at[sp], gate_send.at[1, d], gate_recv.at[1, d], to, dp),
        ]

    def x_copy(kind, c):
        src, dst = ((k_hbm, xk), (v_hbm, xv), (q_hbm, xq))[kind]
        s, h = c // per_seq, (c % per_seq) * PER
        return remote(
            src.at[half * (1 - m) + s, pl.ds(h, PER)],
            dst.at[s, pl.ds(h, PER), here, :],
            x_send.at[kind, c],
            x_recv.at[kind, c],
            mate,
            dp,
        )

    def own_copy():
        return remote(w_hbm, weight.at[dp], own_send.at[0], own_recv.at[0], sp, twin)

    def piece(r):
        return pl.ds(pl.multiple_of(r * rows, rows), rows)

    direct = PIECES - SKIP

    def direct_piece(k):
        return jnp.where(k < SKIP, even * SKIP + k, k + SKIP)

    def wy_copy(j, k):
        r = piece(direct_piece(k))
        return remote(
            w_hbm.at[r],
            weight.at[dp, r],
            wy_send.at[j, k],
            wy_recv.at[j, k],
            sp,
            ((y + j) % chips) * 2 + core,
        )

    def wz_copy(j, k):
        shard = ((y - j + chips) % chips) * 2 + core
        r = piece(direct_piece(k))
        return remote(
            weight.at[shard, r],
            weight.at[shard, r],
            wz_send.at[j, k],
            wz_recv.at[j, k],
            ((g + n_groups - 1) % n_groups) * 2 + m,
            dp,
        )

    def wd_copy(j, r):
        shard = ((y - j + chips) % chips) * 2 + core
        return remote(
            weight.at[shard, piece(r)],
            weight.at[shard, piece(r)],
            wd_send.at[j, r],
            wd_recv.at[j, r],
            sp,
            twin,
        )

    for d in range(1, n_sp):
        for copy in gate_copy(d):
            copy.start()

    @pl.loop(0, chunks)
    def _(c):
        x_copy(0, c).start()
        x_copy(1, c).start()

    @pl.loop(0, direct)
    def _(k):
        for j in range(1, chips):
            wy_copy(j, k).start()

    def mem_copy(member):
        return [
            remote(
                cast.at[pl.ds(half * member, half)],
                mem_in.at[sp],
                mem_send.at[0, member],
                mem_recv.at[0, sp],
                member,
                dp,
            ),
            remote(
                norm_ref.at[pl.ds(half * member, half)],
                norm_in.at[sp],
                mem_send.at[1, member],
                mem_recv.at[1, sp],
                member,
                dp,
            ),
        ]

    def mem_arrived(d):
        return [
            remote(cast.at[mine], mem_in.at[d], mem_send.at[0, 0], mem_recv.at[0, d], d, dp),
            remote(norm_ref.at[mine], norm_in.at[d], mem_send.at[1, 0], mem_recv.at[1, d], d, dp),
        ]

    for member in range(2):

        @pl.when(sp != member)
        def _():
            for copy in mem_copy(member):
                copy.start()

    @pl.loop(0, chunks)
    def _(c):
        x_copy(2, c).start()

    own_copy().start()

    @pl.when(g == 0)
    def _():
        mem_in[sp] = cast[mine]
        norm_in[sp] = norm_ref[mine]

    local[0].wait()
    local[1].wait()
    for d in range(1, n_sp):
        for copy in gate_copy(d):
            copy.wait_recv()

    lane = lax.broadcasted_iota(jnp.int32, (n_groups * items, span), 1)

    def whole(ref):
        return jnp.concatenate(
            [
                jnp.concatenate(
                    [
                        ref[2 * i].astype(f32).reshape(items, tokens),
                        ref[2 * i + 1].astype(f32).reshape(items, tokens),
                    ],
                    axis=1,
                )
                for i in range(n_groups)
            ],
            axis=0,
        )

    gate_in = whole(igr)
    pre = whole(fgr)
    total = jnp.minimum(pre, 0.0) - jnp.log1p(jnp.exp(-jnp.abs(pre)))
    step = 1
    while step < span:
        total = total + jnp.where(lane >= step, pltpu.roll(total, step, 1), 0.0)
        step *= 2
    base = jnp.zeros((items, 1), f32)
    parts = []
    for i in range(n_groups):
        part = total[i * items : (i + 1) * items]
        parts.append(gate_in[i * items : (i + 1) * items] - (part + base))
        base = base + part[:, span - 1 : span]
    offset = jnp.concatenate(parts, axis=0)
    peak = offset
    step = 1
    while step < span:
        peak = jnp.maximum(peak, jnp.where(lane >= step, pltpu.roll(peak, step, 1), FILL))
        step *= 2
    level = level_ref[pl.ds(pl.multiple_of(items * m, items), items), :]
    for i in range(n_groups):
        part = peak[i * items : (i + 1) * items]
        starts[i] = level
        offs[i] = offset[i * items : (i + 1) * items]
        peaks[i] = jnp.maximum(part, level)
        level = jnp.maximum(level, jnp.broadcast_to(part[:, span - 1 : span], part.shape))
    starts[n_groups] = level
    first, last = starts[g], starts[g + 1]
    mine_off = offs[g]
    off_g[...] = mine_off
    wrow[...] = jnp.exp(mine_off - last)
    arow[...] = jnp.exp(first - last)
    srow[...] = first
    columns = jnp.transpose(peaks[g])
    for i in range(items):
        pcol[i] = jnp.broadcast_to(columns[:, i : i + 1], (span, span))

    for copy in local[2:5]:
        copy.wait()

    @pl.when(g == 0)
    def _():
        for d in range(n_sp):

            @pl.when(sp != d)
            def _():
                for copy in mem_arrived(d):
                    copy.wait_recv()

        norm = norm_in[0].reshape(items, width)
        for d in range(1, n_sp):
            norm = norm + norm_in[d].reshape(items, width)
        norm_out[...] = norm

        @pl.loop(0, chunks)
        def _(c):
            s, h = c // per_seq, (c % per_seq) * PER
            for p in range(PER):
                if channels % 16 == 0:
                    st_in[c, p * width : (p + 1) * width] = mem_in[:, s, h + p].reshape(
                        width, width
                    )
                else:
                    for d in range(n_sp):
                        grown[0, d * channels : (d + 1) * channels] = mem_in[d, s, h + p].astype(f32)
                    st_in[c, p * width : (p + 1) * width] = grown[0, 0:width].astype(bf16)
            row = lax.broadcasted_iota(jnp.int32, (TAIL, width), 0)
            tail = jnp.zeros((TAIL, width), f32)
            for p in range(PER):
                tail = jnp.where(row == p, norm_out[pl.ds(c * PER + p, 1), :], tail)
            st_in[c, PER * width :] = tail.astype(bf16)

    tail_row = lax.broadcasted_iota(jnp.int32, (TAIL, width), 0)

    def grow(c):
        x_copy(0, c).wait_recv()
        x_copy(1, c).wait_recv()
        s, h = c // per_seq, (c % per_seq) * PER
        tail = jnp.zeros((TAIL, width), f32)
        for p in range(PER):
            key, value = xk[s, h + p], xv[s, h + p]
            w = wrow[pl.ds(c * PER + p, 1), :]
            scaled = (jnp.transpose(key.astype(f32)) * w).astype(bf16)
            grown[c, p * width : (p + 1) * width] = jnp.dot(
                scaled, value, preferred_element_type=f32
            )
            high = w.astype(bf16).astype(f32)
            both = jnp.where(tail_row == 0, high, jnp.where(tail_row == 1, w - high, 0.0))
            norm = jnp.dot(both.astype(bf16), key, preferred_element_type=f32)
            norm = norm[0:1] + norm[1:2]
            tail = jnp.where(tail_row == p, norm, tail)
        grown[c, PER * width :] = tail

    def st_copy(c):
        return remote(
            st_out.at[c],
            st_in.at[c],
            st_send.at[c],
            st_recv.at[c],
            lax.rem(sp + 2, n_sp),
            dp,
        )

    def chain(c):
        @pl.when(g > 0)
        def _():
            st_copy(c).wait_recv()

        @pl.when(g < n_groups - 1)
        def _():
            tail = jnp.zeros((TAIL, width), f32)
            for p in range(PER):
                part = pl.ds(p * width, width)
                a = arow[pl.ds(c * PER + p, 1), :]
                st_out[c, part] = (st_in[c, part].astype(f32) * a + grown[c, part]).astype(bf16)
                tail = jnp.where(tail_row == p, a, tail)
            part = pl.ds(PER * width, TAIL)
            st_out[c, part] = (st_in[c, part].astype(f32) * tail + grown[c, part]).astype(bf16)
            st_copy(c).start()

    def back_copy(c):
        s, h = c // per_seq, (c % per_seq) * PER
        lanes = pl.ds(pl.multiple_of(h * width, PER * width), PER * width)
        return remote(
            back.at[s, :, lanes],
            act.at[half * m + s, :, lanes],
            back_send.at[c],
            back_recv.at[c],
            mate,
            dp,
        )

    def back_arrived(c):
        s, h = c // per_seq, (c % per_seq) * PER
        lanes = pl.ds(pl.multiple_of(h * width, PER * width), PER * width)
        return remote(
            back.at[s, :, lanes],
            act.at[half * (1 - m) + s, :, lanes],
            back_send.at[c],
            back_recv.at[c],
            mate,
            dp,
        )

    t_row = lax.broadcasted_iota(jnp.int32, (span, span), 0)
    s_col = lax.broadcasted_iota(jnp.int32, (span, span), 1)
    causal = s_col <= t_row
    ones = jnp.ones((span, width), bf16)

    def emit(c):
        x_copy(2, c).wait_recv()
        s, h = c // per_seq, (c % per_seq) * PER
        for p in range(PER):
            i = c * PER + p
            query, key, value = xq[s, h + p], xk[s, h + p], xv[s, h + p]
            memory = st_in[c, p * width : (p + 1) * width]
            norm = jnp.broadcast_to(
                st_in[c, PER * width :].astype(f32)[p : p + 1], (width, width)
            ).astype(bf16)
            raw = lax.dot_general(
                query,
                jnp.concatenate([key, norm], axis=0),
                (((1,), (1,)), ((), ())),
                preferred_element_type=f32,
            )
            column = pcol[i]
            gap = jnp.where(causal, off_g[pl.ds(i, 1), :] - column, FILL)
            scores = (raw[:, :span] * factor * jnp.exp(gap)).astype(bf16)
            weigh = jnp.exp(srow[pl.ds(i, 1), :] - column) * factor
            both = jnp.dot(
                scores, jnp.concatenate([value, ones], axis=1), preferred_element_type=f32
            )
            num = both[:, :width] + weigh * jnp.dot(query, memory, preferred_element_type=f32)
            den = both[:, width:] + weigh * raw[:, span:]
            hidden = (num / jnp.maximum(jnp.abs(den), 1.0)).astype(bf16)
            normed = (hidden.astype(f32) * gain_ref[pl.ds(h + p, 1), :]).astype(bf16)
            top, low = normed[:tokens], normed[tokens:]
            lanes = pl.ds(pl.multiple_of((h + p) * width, width), width)
            act[half * m + s, :, lanes] = jnp.where(m == 0, top, low)
            back[s, :, lanes] = jnp.where(m == 0, low, top)
        back_copy(c).start()

    out_slot = jnp.maximum(chunks, HOP * g)
    slots = max(
        chunks + max(chunks, HOP * (n_groups - 1)),
        2 * (direct - 1) + 2,
        2 * (SKIP - 1) + 7,
    )

    @pl.loop(0, slots)
    def _(t):
        @pl.when(t < chunks)
        def _():
            grow(t)

        c = t - HOP * g

        @pl.when((c >= 0) & (c < chunks))
        def _():
            chain(c)

        o = t - out_slot

        @pl.when((o >= 0) & (o < chunks))
        def _():
            emit(o)

        k = (t - 1) // 2

        @pl.when((t % 2 == 1) & (k < direct))
        def _():
            for j in range(1, chips):
                wy_copy(j, k).wait_recv()
                wd_copy(j, direct_piece(k)).start()

                @pl.when(k < SKIP)
                def _():
                    wz_copy(j, k).start()

        z = (t - 6) // 2

        @pl.when((t >= 6) & (t % 2 == 0) & (z < SKIP))
        def _():
            for j in range(1, chips):
                wz_copy(j, z).wait_recv()
                wd_copy(j, (1 - even) * SKIP + z).start()

    local[5].wait()
    own_copy().wait()
    for j in range(1, chips):

        @pl.loop(0, PIECES)
        def _(r):
            wd_copy(j, r).wait()

    @pl.loop(0, chunks)
    def _(c):
        back_arrived(c).wait_recv()

    left = act[...].reshape(seqs * tokens, heads * width)
    columns_each = weight.shape[2]
    tile = min(512, columns_each)
    tiles = columns_each // tile

    @pl.loop(0, n_dp * tiles)
    def _(n):
        j, b = n // tiles, n % tiles
        shard = (dp + j) % n_dp
        at = pl.ds(pl.multiple_of(b * tile, tile), tile)
        product = jnp.dot(left, weight[shard, :, at], preferred_element_type=f32).astype(bf16)
        out_ref[:, :, pl.ds(pl.multiple_of(shard * columns_each + b * tile, tile), tile)] = (
            product.reshape(seqs, tokens, tile)
        )

    for d in range(1, n_sp):
        for copy in gate_copy(d):
            copy.wait_send()

    @pl.loop(0, chunks)
    def _(c):
        for kind in range(3):
            x_copy(kind, c).wait_send()
        back_copy(c).wait_send()

        @pl.when(g < n_groups - 1)
        def _():
            st_copy(c).wait_send()

    for member in range(2):

        @pl.when(sp != member)
        def _():
            for copy in mem_copy(member):
                copy.wait_send()

    @pl.loop(0, direct)
    def _(k):
        for j in range(1, chips):
            wy_copy(j, k).wait_send()

            @pl.when(k < SKIP)
            def _():
                wz_copy(j, k).wait_send()


def on_device(
    queries,
    keys,
    values,
    input_gate,
    forget_gate,
    start_memory,
    start_norm,
    start_level,
    head_gain,
    out_weight,
):
    seqs, heads, tokens, width = queries.shape
    n_sp, n_dp = lax.axis_size("sp"), lax.axis_size("dp")
    channels = start_memory.shape[2]
    mix, columns = out_weight.shape
    half = seqs // 2
    items = half * heads
    span = 2 * tokens
    groups = n_sp // 2
    chips = n_dp // 2
    chunks = items // PER
    direct = PIECES - SKIP
    f32, bf16 = jnp.float32, jnp.bfloat16
    level = jnp.broadcast_to(start_level.reshape(seqs * heads, 1), (seqs * heads, span))
    place = lax.axis_index("sp") * channels
    norm = lax.dynamic_update_slice(
        jnp.zeros((seqs, heads, width), f32), start_norm, (0, 0, place)
    )
    sizes = (n_sp, n_dp, seqs, heads, tokens, width, channels)
    any_spec = pl.BlockSpec(memory_space=pl.ANY)
    vmem = pl.BlockSpec(memory_space=pltpu.VMEM)
    dma = pltpu.SemaphoreType.DMA
    return pl.pallas_call(
        lambda *refs: layer_kernel(sizes, *refs),
        out_shape=jax.ShapeDtypeStruct((seqs, tokens, n_dp * columns), bf16),
        in_specs=[any_spec] * 6 + [vmem] * 4,
        out_specs=vmem,
        scratch_shapes=[
            pltpu.VMEM((half, heads, span, width), bf16),
            pltpu.VMEM((half, heads, span, width), bf16),
            pltpu.VMEM((half, heads, span, width), bf16),
            pltpu.VMEM((n_sp, half, heads, tokens), bf16),
            pltpu.VMEM((n_sp, half, heads, tokens), bf16),
            pltpu.VMEM((seqs, heads, channels, width), bf16),
            pltpu.VMEM((n_sp, half, heads, channels, width), bf16),
            pltpu.VMEM((n_sp, half, heads, width), f32),
            pltpu.VMEM((items, width), f32),
            pltpu.VMEM((groups, items, span), f32),
            pltpu.VMEM((groups, items, span), f32),
            pltpu.VMEM((groups + 1, items, span), f32),
            pltpu.VMEM((items, span), f32),
            pltpu.VMEM((items, span), f32),
            pltpu.VMEM((items, span), f32),
            pltpu.VMEM((items, span), f32),
            pltpu.VMEM((items, span, span), f32),
            pltpu.VMEM((chunks, PER * width + TAIL, width), f32),
            pltpu.VMEM((chunks, PER * width + TAIL, width), bf16),
            pltpu.VMEM((chunks, PER * width + TAIL, width), bf16),
            pltpu.VMEM((seqs, tokens, heads * width), bf16),
            pltpu.VMEM((half, tokens, heads * width), bf16),
            pltpu.VMEM((n_dp, mix, columns), bf16),
            dma((6,)),
            dma((2, n_sp)),
            dma((2, n_sp)),
            dma((3, chunks)),
            dma((3, chunks)),
            dma((2, 2)),
            dma((2, n_sp)),
            dma((chunks,)),
            dma((chunks,)),
            dma((chunks,)),
            dma((chunks,)),
            dma((chips, direct)),
            dma((chips, direct)),
            dma((chips, SKIP)),
            dma((chips, SKIP)),
            dma((chips, PIECES)),
            dma((chips, PIECES)),
            dma((1,)),
            dma((1,)),
        ],
        compiler_params=pltpu.CompilerParams(
            collective_id=0, has_side_effects=True, vmem_limit_bytes=40 * 1024 * 1024
        ),
        name="layer",
    )(
        queries,
        keys,
        values,
        input_gate,
        forget_gate,
        out_weight,
        start_memory,
        norm,
        level,
        head_gain,
    )


def solution(mesh):
    in_specs = (
        P("dp", None, "sp", None),
        P("dp", None, "sp", None),
        P("dp", None, "sp", None),
        P("dp", None, "sp"),
        P("dp", None, "sp"),
        P("dp", None, "sp", None),
        P("dp", None, "sp"),
        P("dp", None),
        P(),
        P(None, "dp"),
    )
    out_specs = P("dp", "sp", None)
    return jax.shard_map(
        on_device, mesh=mesh, in_specs=in_specs, out_specs=out_specs, check_vma=False
    )
```

time: 99 us -> 84.6 us (0.85)
  the two profiles are of different devices: /device:TPU:0 before, /device:TPU:11 now
where the time goes in v1:
time: 84.6 us; the launch traced here: 84.1 us
  Pallas kernels  72.9 us (86%)
  local copies, waits for them, and re-layouts  11.2 us (13%)
    pallas_call x1, Pallas kernels, on_device(): pl.pallas_call(lambda *refs: layer_kernel(sizes, *refs), out_shape=jax.Sh...  72.9 us
    unnamed x17, local copies, waits for them, and re-layouts  9.07 us

profile of v1, /device:TPU:11, one launch (start us, length us, event | category | flops | bytes accessed | tf_op | source)
XLA Modules:
  0.0 84.1 jit_solution(14700326478837368551)
XLA Ops:
  0.0 0.8 broadcast_in_dim.11
  0.8 0.1 broadcast_in_dim.12.refs_8_
  0.8 1.3 %dynamic_update_slice.3.refs_7_ = f32[4,8,128]{2,1,0:T(8,128)S(1)} dynamic-update-slice(f32[4,8,128]{2,1,0:T(8,128)S(1)} %broadcast_in_dim.10, f32[4,8,16]{2,1,0:T(8,128)} %param.16, s32[]{:T(128)} %constant.3.clone.1, s32[]{:T(128)} %constant.3.clone.1, s32[]{:T(128)S(6)} %select_n.3) | dynamic-update-slice | bytes 4100 | tf_op jit(solution)/shard_map/dynamic_update_slice | solution.py:583
  2.1 0.0 copy-start
  2.2 1.6 %copy-done = bf16[1024,1024]{1,0:T(8,128)(2,1)S(1)} copy-done((bf16[1024,1024]{1,0:T(8,128)(2,1)S(1)}, bf16[1024,1024]{1,0:T(8,128)(2,1)}, u32[]{:S(2)}) %copy-start) | copy-done | bytes 2097176
  3.7 0.0 copy-start.1
  3.7 1.0 %copy-done.1 = bf16[4,8,64,128]{3,2,1,0:T(8,128)(2,1)S(1)} copy-done((bf16[4,8,64,128]{3,2,1,0:T(8,128)(2,1)S(1)}, bf16[4,8,64,128]{3,2,1,0:T(8,128)(2,1)}, u32[]{:S(2)}) %copy-start.1) | copy-done | bytes 524312
  4.8 0.0 copy-start.2
  4.8 1.0 %copy-done.2 = bf16[4,8,64,128]{3,2,1,0:T(8,128)(2,1)S(1)} copy-done((bf16[4,8,64,128]{3,2,1,0:T(8,128)(2,1)S(1)}, bf16[4,8,64,128]{3,2,1,0:T(8,128)(2,1)}, u32[]{:S(2)}) %copy-start.2) | copy-done | bytes 524312
  5.8 0.0 copy-start.3
  5.8 1.0 %copy-done.3 = bf16[4,8,64,128]{3,2,1,0:T(8,128)(2,1)S(1)} copy-done((bf16[4,8,64,128]{3,2,1,0:T(8,128)(2,1)S(1)}, bf16[4,8,64,128]{3,2,1,0:T(8,128)(2,1)}, u32[]{:S(2)}) %copy-start.3) | copy-done | bytes 524312
  6.9 0.0 copy-start.4
  6.9 0.9 %copy-done.4 = f32[4,8,16,128]{3,2,1,0:T(8,128)S(1)} copy-done((f32[4,8,16,128]{3,2,1,0:T(8,128)S(1)}, f32[4,8,16,128]{3,2,1,0:T(8,128)}, u32[]{:S(2)}) %copy-start.4) | copy-done | bytes 262168
  7.8 0.0 copy-start.5
  7.8 0.7 copy-done.5
  8.5 0.0 copy-start.6
  8.5 0.7 copy-done.6
  9.2 0.0 copy-start.7
  9.2 0.7 copy-done.7
  9.9 72.9 %layer.1 = bf16[4,64,4096]{2,1,0:T(8,128)(2,1)S(1)} custom-call(bf16[4,8,64,128]{3,2,1,0:T(8,128)(2,1)S(1)} %copy-done.1, bf16[4,8,64,128]{3,2,1,0:T(8,128)(2,1)S(1)} %copy-done.2, bf16[4,8,64,128]{3,2,1,0:T(8,128)(2,1)S(1)} %copy-done.3, bf16[4,8,64]{2,1,0:T(8,128)(2,1)S(1)} %copy-done.5, bf16[4,8,64]{2,1,0:T(8,128)(2,1)S(1)} %copy-done.6, ...), custom_call_target="tpu_custom_call" | custom-call | tf_op jit(solution)/shard_map/layer/pallas_call | solution.py:590
  82.8 1.3 %copy.13 = bf16[4,64,4096]{2,1,0:T(8,128)(2,1)} copy(bf16[4,64,4096]{2,1,0:T(8,128)(2,1)S(1)} %layer.1) | data formatting | bytes 4194304
  (1 shorter events, 0.0 us)
Async XLA Ops:
  2.1 1.6 %copy-start = (bf16[1024,1024]{1,0:T(8,128)(2,1)S(1)}, bf16[1024,1024]{1,0:T(8,128)(2,1)}, u32[]{:S(2)}) copy-start(bf16[1024,1024]{1,0:T(8,128)(2,1)} %refs_5_.1) | copy-start | bytes 6291460
  3.7 1.0 %copy-start.1 = (bf16[4,8,64,128]{3,2,1,0:T(8,128)(2,1)S(1)}, bf16[4,8,64,128]{3,2,1,0:T(8,128)(2,1)}, u32[]{:S(2)}) copy-start(bf16[4,8,64,128]{3,2,1,0:T(8,128)(2,1)} %refs_0_.1) | copy-start | bytes 1572868
  4.8 1.0 %copy-start.2 = (bf16[4,8,64,128]{3,2,1,0:T(8,128)(2,1)S(1)}, bf16[4,8,64,128]{3,2,1,0:T(8,128)(2,1)}, u32[]{:S(2)}) copy-start(bf16[4,8,64,128]{3,2,1,0:T(8,128)(2,1)} %refs_1_.1) | copy-start | bytes 1572868
  5.8 1.0 %copy-start.3 = (bf16[4,8,64,128]{3,2,1,0:T(8,128)(2,1)S(1)}, bf16[4,8,64,128]{3,2,1,0:T(8,128)(2,1)}, u32[]{:S(2)}) copy-start(bf16[4,8,64,128]{3,2,1,0:T(8,128)(2,1)} %refs_2_.1) | copy-start | bytes 1572868
  6.9 0.9 %copy-start.4 = (f32[4,8,16,128]{3,2,1,0:T(8,128)S(1)}, f32[4,8,16,128]{3,2,1,0:T(8,128)}, u32[]{:S(2)}) copy-start(f32[4,8,16,128]{3,2,1,0:T(8,128)} %refs_6_.1) | copy-start | bytes 786436
  7.8 0.7 copy-start.5
  8.5 0.7 copy-start.6
  9.2 0.7 copy-start.7

commit v2 on v1

--- a/solution.py
+++ b/solution.py
@@ -10,7 +10,7 @@
 PER = 2
 HOP = 3
 PIECES = 16
-SKIP = 7
+SKIP = 6
 TAIL = 16
 
 
@@ -22,11 +22,16 @@
     ig_hbm,
     fg_hbm,
     w_hbm,
+    mem_hbm,
+    norm_hbm,
+    level_hbm,
+    gain_hbm,
+    out_ref,
     mem_ref,
-    norm_ref,
+    norm_raw,
     level_ref,
     gain_ref,
-    out_ref,
+    norm_ref,
     xq,
     xk,
     xv,
@@ -36,6 +41,7 @@
     mem_in,
     norm_in,
     norm_out,
+    whole_ref,
     offs,
     peaks,
     starts,
@@ -57,6 +63,8 @@
     x_recv,
     mem_send,
     mem_recv,
+    norm_send,
+    norm_recv,
     st_send,
     st_recv,
     back_send,
@@ -64,6 +72,7 @@
     wy_send,
     wy_recv,
     wz_send,
+    wu_send,
     wz_recv,
     wd_send,
     wd_recv,
@@ -107,7 +116,11 @@
         pltpu.make_async_copy(k_hbm.at[mine], xk.at[:, :, here, :], loc_sem.at[2]),
         pltpu.make_async_copy(v_hbm.at[mine], xv.at[:, :, here, :], loc_sem.at[3]),
         pltpu.make_async_copy(q_hbm.at[mine], xq.at[:, :, here, :], loc_sem.at[4]),
-        pltpu.make_async_copy(w_hbm, weight.at[dp], loc_sem.at[5]),
+        pltpu.make_async_copy(mem_hbm, mem_ref, loc_sem.at[5]),
+        pltpu.make_async_copy(norm_hbm, norm_raw, loc_sem.at[6]),
+        pltpu.make_async_copy(level_hbm, level_ref, loc_sem.at[7]),
+        pltpu.make_async_copy(gain_hbm, gain_ref, loc_sem.at[8]),
+        pltpu.make_async_copy(w_hbm, weight.at[dp], loc_sem.at[9]),
     ]
     for copy in local:
         copy.start()
@@ -120,7 +133,14 @@
         pl.semaphore_signal(
             barrier, inc=1, device_id=(sp, ((y + j) % chips) * 2 + core), device_id_type=MESH
         )
+    local[5].wait()
     cast[...] = mem_ref[...].astype(bf16)
+    local[6].wait()
+    norm_ref[...] = jnp.zeros((seqs, heads, width), f32)
+    norm_ref[:, :, 0:channels] = norm_raw[...]
+    norm_ref[...] = pltpu.roll(
+        norm_ref[...].reshape(seqs * heads, width), sp * channels, 1
+    ).reshape(seqs, heads, width)
     pl.semaphore_wait(barrier, n_sp - 1 + 1 + chips - 1)
 
     def gate_copy(d):
@@ -165,17 +185,27 @@
             ((y + j) % chips) * 2 + core,
         )
 
-    def wz_copy(j, k):
+    def wz_copy(j, k, down=True):
         shard = ((y - j + chips) % chips) * 2 + core
         r = piece(direct_piece(k))
+        to = lax.rem(sp + n_sp - 2, n_sp) if down else lax.rem(sp + 2, n_sp)
         return remote(
             weight.at[shard, r],
             weight.at[shard, r],
-            wz_send.at[j, k],
+            (wz_send if down else wu_send).at[j, k],
             wz_recv.at[j, k],
-            ((g + n_groups - 1) % n_groups) * 2 + m,
+            to,
             dp,
         )
+
+    def wz_each(j, k, act):
+        @pl.when(g > 0)
+        def _():
+            act(wz_copy(j, k))
+
+        @pl.when(g == n_groups - 2)
+        def _():
+            act(wz_copy(j, k, down=False))
 
     def wd_copy(j, r):
         shard = ((y - j + chips) % chips) * 2 + core
@@ -192,6 +222,57 @@
         for copy in gate_copy(d):
             copy.start()
 
+    def mem_copy(member, c):
+        s, h = c // per_seq, (c % per_seq) * PER
+        return remote(
+            cast.at[half * member + s, pl.ds(h, PER)],
+            mem_in.at[sp, s, pl.ds(h, PER)],
+            mem_send.at[member, c],
+            mem_recv.at[sp, c],
+            member,
+            dp,
+        )
+
+    def mem_arrived(d, c):
+        s, h = c // per_seq, (c % per_seq) * PER
+        return remote(
+            cast.at[half * m + s, pl.ds(h, PER)],
+            mem_in.at[d, s, pl.ds(h, PER)],
+            mem_send.at[0, c],
+            mem_recv.at[d, c],
+            d,
+            dp,
+        )
+
+    def norm_copy(member):
+        return remote(
+            norm_ref.at[pl.ds(half * member, half)],
+            norm_in.at[sp],
+            norm_send.at[member],
+            norm_recv.at[sp],
+            member,
+            dp,
+        )
+
+    def norm_arrived(d):
+        return remote(
+            norm_ref.at[mine], norm_in.at[d], norm_send.at[0], norm_recv.at[d], d, dp
+        )
+
+    for member in range(2):
+
+        @pl.when(sp != member)
+        def _():
+            norm_copy(member).start()
+
+    @pl.loop(0, chunks)
+    def _(c):
+        for member in range(2):
+
+            @pl.when(sp != member)
+            def _():
+                mem_copy(member, c).start()
+
     @pl.loop(0, chunks)
     def _(c):
         x_copy(0, c).start()
@@ -201,39 +282,6 @@
     def _(k):
         for j in range(1, chips):
             wy_copy(j, k).start()
-
-    def mem_copy(member):
-        return [
-            remote(
-                cast.at[pl.ds(half * member, half)],
-                mem_in.at[sp],
-                mem_send.at[0, member],
-                mem_recv.at[0, sp],
-                member,
-                dp,
-            ),
-            remote(
-                norm_ref.at[pl.ds(half * member, half)],
-                norm_in.at[sp],
-                mem_send.at[1, member],
-                mem_recv.at[1, sp],
-                member,
-                dp,
-            ),
-        ]
-
-    def mem_arrived(d):
-        return [
-            remote(cast.at[mine], mem_in.at[d], mem_send.at[0, 0], mem_recv.at[0, d], d, dp),
-            remote(norm_ref.at[mine], norm_in.at[d], mem_send.at[1, 0], mem_recv.at[1, d], d, dp),
-        ]
-
-    for member in range(2):
-
-        @pl.when(sp != member)
-        def _():
-            for copy in mem_copy(member):
-                copy.start()
 
     @pl.loop(0, chunks)
     def _(c):
@@ -288,7 +336,21 @@
     while step < span:
         peak = jnp.maximum(peak, jnp.where(lane >= step, pltpu.roll(peak, step, 1), FILL))
         step *= 2
-    level = level_ref[pl.ds(pl.multiple_of(items * m, items), items), :]
+    local[7].wait()
+    local[8].wait()
+    eye = lax.broadcasted_iota(jnp.int32, (heads, heads), 0) == lax.broadcasted_iota(
+        jnp.int32, (heads, heads), 1
+    )
+    level = jnp.concatenate(
+        [
+            jnp.sum(
+                jnp.where(eye, level_ref[pl.ds(half * m + i, 1), :], 0.0), axis=1, keepdims=True
+            )
+            for i in range(half)
+        ],
+        axis=0,
+    )
+    level = jnp.broadcast_to(level, (items, span))
     for i in range(n_groups):
         part = peak[i * items : (i + 1) * items]
         starts[i] = level
@@ -308,38 +370,6 @@
 
     for copy in local[2:5]:
         copy.wait()
-
-    @pl.when(g == 0)
-    def _():
-        for d in range(n_sp):
-
-            @pl.when(sp != d)
-            def _():
-                for copy in mem_arrived(d):
-                    copy.wait_recv()
-
-        norm = norm_in[0].reshape(items, width)
-        for d in range(1, n_sp):
-            norm = norm + norm_in[d].reshape(items, width)
-        norm_out[...] = norm
-
-        @pl.loop(0, chunks)
-        def _(c):
-            s, h = c // per_seq, (c % per_seq) * PER
-            for p in range(PER):
-                if channels % 16 == 0:
-                    st_in[c, p * width : (p + 1) * width] = mem_in[:, s, h + p].reshape(
-                        width, width
-                    )
-                else:
-                    for d in range(n_sp):
-                        grown[0, d * channels : (d + 1) * channels] = mem_in[d, s, h + p].astype(f32)
-                    st_in[c, p * width : (p + 1) * width] = grown[0, 0:width].astype(bf16)
-            row = lax.broadcasted_iota(jnp.int32, (TAIL, width), 0)
-            tail = jnp.zeros((TAIL, width), f32)
-            for p in range(PER):
-                tail = jnp.where(row == p, norm_out[pl.ds(c * PER + p, 1), :], tail)
-            st_in[c, PER * width :] = tail.astype(bf16)
 
     tail_row = lax.broadcasted_iota(jnp.int32, (TAIL, width), 0)
 
@@ -372,7 +402,43 @@
             dp,
         )
 
+    def seed(c):
+        for d in range(n_sp):
+
+            @pl.when(sp != d)
+            def _():
+                mem_arrived(d, c).wait_recv()
+
+        @pl.when(c == 0)
+        def _():
+            for d in range(n_sp):
+
+                @pl.when(sp != d)
+                def _():
+                    norm_arrived(d).wait_recv()
+
+            norm = norm_in[0].reshape(items, width)
+            for d in range(1, n_sp):
+                norm = norm + norm_in[d].reshape(items, width)
+            norm_out[...] = norm
+
+        s, h = c // per_seq, (c % per_seq) * PER
+        tail = jnp.zeros((TAIL, width), f32)
+        for p in range(PER):
+            if channels % 16 == 0:
+                st_in[c, p * width : (p + 1) * width] = mem_in[:, s, h + p].reshape(width, width)
+            else:
+                for d in range(n_sp):
+                    whole_ref[d * channels : (d + 1) * channels] = mem_in[d, s, h + p].astype(f32)
+                st_in[c, p * width : (p + 1) * width] = whole_ref[...].astype(bf16)
+            tail = jnp.where(tail_row == p, norm_out[pl.ds(c * PER + p, 1), :], tail)
+        st_in[c, PER * width :] = tail.astype(bf16)
+
     def chain(c):
+        @pl.when(g == 0)
+        def _():
+            seed(c)
+
         @pl.when(g > 0)
         def _():
             st_copy(c).wait_recv()
@@ -452,11 +518,11 @@
         back_copy(c).start()
 
     out_slot = jnp.maximum(chunks, HOP * g)
-    slots = max(
-        chunks + max(chunks, HOP * (n_groups - 1)),
-        2 * (direct - 1) + 2,
-        2 * (SKIP - 1) + 7,
-    )
+    slots = max(chunks + max(chunks, HOP * (n_groups - 1)), 2 * SKIP)
+
+    def pass_on(j, k):
+        wy_copy(j, k).wait_recv()
+        wd_copy(j, direct_piece(k)).start()
 
     @pl.loop(0, slots)
     def _(t):
@@ -470,39 +536,34 @@
         def _():
             chain(c)
 
+        k = (t - 1) // 2
+
+        @pl.when((t % 2 == 1) & (k < SKIP))
+        def _():
+            for j in range(1, chips):
+                pass_on(j, k)
+                wz_each(j, k, lambda copy: copy.start())
+
         o = t - out_slot
 
         @pl.when((o >= 0) & (o < chunks))
         def _():
             emit(o)
 
-        k = (t - 1) // 2
-
-        @pl.when((t % 2 == 1) & (k < direct))
-        def _():
+    def pass_up_to(first, last):
+        @pl.loop(first, last)
+        def _(k):
             for j in range(1, chips):
-                wy_copy(j, k).wait_recv()
-                wd_copy(j, direct_piece(k)).start()
-
-                @pl.when(k < SKIP)
-                def _():
-                    wz_copy(j, k).start()
-
-        z = (t - 6) // 2
-
-        @pl.when((t >= 6) & (t % 2 == 0) & (z < SKIP))
-        def _():
-            for j in range(1, chips):
-                wz_copy(j, z).wait_recv()
-                wd_copy(j, (1 - even) * SKIP + z).start()
-
-    local[5].wait()
-    own_copy().wait()
-    for j in range(1, chips):
-
-        @pl.loop(0, PIECES)
-        def _(r):
-            wd_copy(j, r).wait()
+                pass_on(j, k)
+
+    @pl.loop(0, SKIP)
+    def _(k):
+        for j in range(1, chips):
+            wz_copy(j, k).wait_recv()
+            wd_copy(j, (1 - even) * SKIP + k).start()
+
+    middle = (SKIP + direct) // 2
+    pass_up_to(SKIP, middle)
 
     @pl.loop(0, chunks)
     def _(c):
@@ -513,15 +574,28 @@
     tile = min(512, columns_each)
     tiles = columns_each // tile
 
-    @pl.loop(0, n_dp * tiles)
-    def _(n):
-        j, b = n // tiles, n % tiles
-        shard = (dp + j) % n_dp
-        at = pl.ds(pl.multiple_of(b * tile, tile), tile)
-        product = jnp.dot(left, weight[shard, :, at], preferred_element_type=f32).astype(bf16)
-        out_ref[:, :, pl.ds(pl.multiple_of(shard * columns_each + b * tile, tile), tile)] = (
-            product.reshape(seqs, tokens, tile)
-        )
+    def project(shard):
+        @pl.loop(0, tiles)
+        def _(b):
+            at = pl.ds(pl.multiple_of(b * tile, tile), tile)
+            product = jnp.dot(left, weight[shard, :, at], preferred_element_type=f32)
+            out_ref[:, :, pl.ds(pl.multiple_of(shard * columns_each + b * tile, tile), tile)] = (
+                product.astype(bf16).reshape(seqs, tokens, tile)
+            )
+
+    local[9].wait()
+    project(dp)
+    own_copy().wait()
+    project(twin)
+    pass_up_to(middle, direct)
+    for j in range(1, chips):
+        project(((y - j + chips) % chips) * 2 + core)
+
+        @pl.loop(0, PIECES)
+        def _(r):
+            wd_copy(j, r).wait()
+
+        project(((y - j + chips) % chips) * 2 + 1 - core)
 
     for d in range(1, n_sp):
         for copy in gate_copy(d):
@@ -541,8 +615,11 @@
 
         @pl.when(sp != member)
         def _():
-            for copy in mem_copy(member):
-                copy.wait_send()
+            norm_copy(member).wait_send()
+
+            @pl.loop(0, chunks)
+            def _(c):
+                mem_copy(member, c).wait_send()
 
     @pl.loop(0, direct)
     def _(k):
@@ -551,7 +628,7 @@
 
             @pl.when(k < SKIP)
             def _():
-                wz_copy(j, k).wait_send()
+                wz_each(j, k, lambda copy: copy.wait_send())
 
 
 def on_device(
@@ -578,21 +655,36 @@
     chunks = items // PER
     direct = PIECES - SKIP
     f32, bf16 = jnp.float32, jnp.bfloat16
-    level = jnp.broadcast_to(start_level.reshape(seqs * heads, 1), (seqs * heads, span))
-    place = lax.axis_index("sp") * channels
-    norm = lax.dynamic_update_slice(
-        jnp.zeros((seqs, heads, width), f32), start_norm, (0, 0, place)
-    )
     sizes = (n_sp, n_dp, seqs, heads, tokens, width, channels)
-    any_spec = pl.BlockSpec(memory_space=pl.ANY)
+    operands = [
+        pltpu.with_memory_space_constraint(array, pltpu.HBM)
+        for array in (
+            queries,
+            keys,
+            values,
+            input_gate,
+            forget_gate,
+            out_weight,
+            start_memory,
+            start_norm,
+            start_level,
+            head_gain,
+        )
+    ]
+    hbm_spec = pl.BlockSpec(memory_space=pltpu.HBM)
     vmem = pl.BlockSpec(memory_space=pltpu.VMEM)
     dma = pltpu.SemaphoreType.DMA
     return pl.pallas_call(
         lambda *refs: layer_kernel(sizes, *refs),
         out_shape=jax.ShapeDtypeStruct((seqs, tokens, n_dp * columns), bf16),
-        in_specs=[any_spec] * 6 + [vmem] * 4,
+        in_specs=[hbm_spec] * len(operands),
         out_specs=vmem,
         scratch_shapes=[
+            pltpu.VMEM((seqs, heads, channels, width), f32),
+            pltpu.VMEM((seqs, heads, channels), f32),
+            pltpu.VMEM((seqs, heads), f32),
+            pltpu.VMEM((heads, width), f32),
+            pltpu.VMEM((seqs, heads, width), f32),
             pltpu.VMEM((half, heads, span, width), bf16),
             pltpu.VMEM((half, heads, span, width), bf16),
             pltpu.VMEM((half, heads, span, width), bf16),
@@ -602,6 +694,7 @@
             pltpu.VMEM((n_sp, half, heads, channels, width), bf16),
             pltpu.VMEM((n_sp, half, heads, width), f32),
             pltpu.VMEM((items, width), f32),
+            pltpu.VMEM((width, width), f32),
             pltpu.VMEM((groups, items, span), f32),
             pltpu.VMEM((groups, items, span), f32),
             pltpu.VMEM((groups + 1, items, span), f32),
@@ -616,19 +709,22 @@
             pltpu.VMEM((seqs, tokens, heads * width), bf16),
             pltpu.VMEM((half, tokens, heads * width), bf16),
             pltpu.VMEM((n_dp, mix, columns), bf16),
-            dma((6,)),
+            dma((10,)),
             dma((2, n_sp)),
             dma((2, n_sp)),
             dma((3, chunks)),
             dma((3, chunks)),
-            dma((2, 2)),
-            dma((2, n_sp)),
+            dma((2, chunks)),
+            dma((n_sp, chunks)),
+            dma((2,)),
+            dma((n_sp,)),
             dma((chunks,)),
             dma((chunks,)),
             dma((chunks,)),
             dma((chunks,)),
             dma((chips, direct)),
             dma((chips, direct)),
+            dma((chips, SKIP)),
             dma((chips, SKIP)),
             dma((chips, SKIP)),
             dma((chips, PIECES)),
@@ -640,18 +736,7 @@
             collective_id=0, has_side_effects=True, vmem_limit_bytes=40 * 1024 * 1024
         ),
         name="layer",
-    )(
-        queries,
-        keys,
-        values,
-        input_gate,
-        forget_gate,
-        out_weight,
-        start_memory,
-        norm,
-        level,
-        head_gain,
-    )
+    )(*operands)
 
 
 def solution(mesh):

time: 84.6 us -> 53.5 us (0.63)
  the two profiles are of different devices: /device:TPU:11 before, /device:TPU:29 now
where the time goes in v2:
time: 53.5 us; the launch traced here: 53.4 us
  Pallas kernels  52.1 us (97%)
  local copies, waits for them, and re-layouts  1.32 us (2%)
    pallas_call x1, Pallas kernels, on_device(): pl.pallas_call(lambda *refs: layer_kernel(sizes, *refs), out_shape=jax.Sh...  52.1 us
    unnamed x1, local copies, waits for them, and re-layouts  1.32 us

profile of v2, /device:TPU:29, one launch (start us, length us, event | category | flops | bytes accessed | tf_op | source)
XLA Modules:
  0.0 53.4 jit_solution(11732339365704466454)
XLA Ops:
  0.0 52.1 %layer.1 = bf16[4,64,4096]{2,1,0:T(8,128)(2,1)S(1)} custom-call(bf16[4,8,64,128]{3,2,1,0:T(8,128)(2,1)} %refs_0_.1, bf16[4,8,64,128]{3,2,1,0:T(8,128)(2,1)} %refs_1_.1, bf16[4,8,64,128]{3,2,1,0:T(8,128)(2,1)} %refs_2_.1, bf16[4,8,64]{2,1,0:T(8,128)(2,1)} %refs_3_.1, bf16[4,8,64]{2,1,0:T(8,128)(2,1)} %refs_4_.1, bf16[1024,1024]{1,0:T(8,128)(2,1)} %refs_5_.1, ...), custom_call_target="tpu_custom_call" | custom-call | tf_op jit(solution)/shard_map/layer/pallas_call | solution.py:677
  52.1 1.3 %copy.12 = bf16[4,64,4096]{2,1,0:T(8,128)(2,1)} copy(bf16[4,64,4096]{2,1,0:T(8,128)(2,1)S(1)} %layer.1) | data formatting | bytes 4194304

commit v3 on v2

--- a/solution.py
+++ b/solution.py
@@ -10,7 +10,14 @@
 PER = 2
 HOP = 3
 PIECES = 16
-SKIP = 6
+SKIP = 5
+SIDE = 2
+WHEN = (0, 1, 3, 4, 6, 8, 10, 12, 14)
+LATE = (8, 8, 8, 8, 10, 12, 15, 16, 16)
+WHEN_SKIP = 13
+WHEN_SIDE = 15
+OWN_SLOTS = 3
+WHEN_OWN = 14
 TAIL = 16
 
 
@@ -62,6 +69,7 @@
     x_send,
     x_recv,
     mem_send,
+    cross_recv,
     mem_recv,
     norm_send,
     norm_recv,
@@ -74,6 +82,8 @@
     wz_send,
     wu_send,
     wz_recv,
+    wx_send,
+    wx_recv,
     wd_send,
     wd_recv,
     own_send,
@@ -108,6 +118,9 @@
             device_id_type=MESH,
         )
 
+    def arrived(ref, sem):
+        pltpu.make_async_copy(ref, ref, sem).wait()
+
     mine = pl.ds(half * m, half)
     here = pl.ds(pl.multiple_of(m * tokens, tokens), tokens)
     local = [
@@ -147,8 +160,8 @@
         to = (sp + d) % n_sp
         part = pl.ds(half * (to % 2), half)
         return [
-            remote(ig_hbm.at[part], igr.at[sp], gate_send.at[0, d], gate_recv.at[0, d], to, dp),
-            remote(fg_hbm.at[part], fgr.at[sp], gate_send.at[1, d], gate_recv.at[1, d], to, dp),
+            remote(ig_hbm.at[part], igr.at[sp], gate_send.at[0], gate_recv.at[0], to, dp),
+            remote(fg_hbm.at[part], fgr.at[sp], gate_send.at[1], gate_recv.at[1], to, dp),
         ]
 
     def x_copy(kind, c):
@@ -157,8 +170,8 @@
         return remote(
             src.at[half * (1 - m) + s, pl.ds(h, PER)],
             dst.at[s, pl.ds(h, PER), here, :],
-            x_send.at[kind, c],
-            x_recv.at[kind, c],
+            x_send.at[kind],
+            x_recv.at[kind // 2, c],
             mate,
             dp,
         )
@@ -169,17 +182,20 @@
     def piece(r):
         return pl.ds(pl.multiple_of(r * rows, rows), rows)
 
-    direct = PIECES - SKIP
+    direct = PIECES - SKIP - SIDE
 
     def direct_piece(k):
-        return jnp.where(k < SKIP, even * SKIP + k, k + SKIP)
+        side = 2 * SKIP + (1 - m) * SIDE + k - SKIP
+        return jnp.where(
+            k < SKIP, even * SKIP + k, jnp.where(k < SKIP + SIDE, side, k + SKIP + SIDE)
+        )
 
     def wy_copy(j, k):
         r = piece(direct_piece(k))
         return remote(
             w_hbm.at[r],
             weight.at[dp, r],
-            wy_send.at[j, k],
+            wy_send.at[j],
             wy_recv.at[j, k],
             sp,
             ((y + j) % chips) * 2 + core,
@@ -192,93 +208,126 @@
         return remote(
             weight.at[shard, r],
             weight.at[shard, r],
-            (wz_send if down else wu_send).at[j, k],
-            wz_recv.at[j, k],
+            (wz_send if down else wu_send).at[j],
+            wz_recv.at[j],
             to,
             dp,
         )
 
-    def wz_each(j, k, act):
+    def wz_each(j, k, do):
         @pl.when(g > 0)
         def _():
-            act(wz_copy(j, k))
+            do(wz_copy(j, k))
 
         @pl.when(g == n_groups - 2)
         def _():
-            act(wz_copy(j, k, down=False))
+            do(wz_copy(j, k, down=False))
+
+    def wx_copy(j, k):
+        shard = ((y - j + chips) % chips) * 2 + core
+        r = piece(direct_piece(k))
+        return remote(
+            weight.at[shard, r],
+            weight.at[shard, r],
+            wx_send.at[j],
+            wx_recv.at[j],
+            mate,
+            dp,
+        )
 
     def wd_copy(j, r):
         shard = ((y - j + chips) % chips) * 2 + core
         return remote(
             weight.at[shard, piece(r)],
             weight.at[shard, piece(r)],
-            wd_send.at[j, r],
-            wd_recv.at[j, r],
+            wd_send.at[j],
+            wd_recv.at[j],
             sp,
             twin,
         )
 
+    def mem_part(e):
+        return e // 2, pl.ds((e % 2) * (heads // 2), heads // 2)
+
+    def mem_cross(e):
+        s, h = mem_part(e)
+        return remote(
+            cast.at[half * (1 - m) + s, h],
+            mem_in.at[sp, s, h],
+            mem_send.at[0],
+            cross_recv.at[e],
+            mate,
+            dp,
+        )
+
+    def mem_cross_arrived(e):
+        s, h = mem_part(e)
+        return remote(
+            cast.at[half * (1 - m) + s, h],
+            mem_in.at[mate, s, h],
+            mem_send.at[0],
+            cross_recv.at[e],
+            mate,
+            dp,
+        )
+
+    def mem_own(e):
+        s, h = mem_part(e)
+        return remote(
+            cast.at[half * m + s, h],
+            mem_in.at[sp, s, h],
+            mem_send.at[1],
+            mem_recv.at[e],
+            m,
+            dp,
+        )
+
+    def mem_mate(e):
+        s, h = mem_part(e)
+        return remote(
+            mem_in.at[mate, s, h],
+            mem_in.at[mate, s, h],
+            mem_send.at[2],
+            mem_recv.at[e],
+            m,
+            dp,
+        )
+
+    def norm_copy(member):
+        return remote(
+            norm_ref.at[pl.ds(half * member, half)],
+            norm_in.at[sp],
+            norm_send.at[member],
+            norm_recv.at[0],
+            member,
+            dp,
+        )
+
+    for k in range(2):
+        for j in range(1, chips):
+            wy_copy(j, k).start()
+    for e in range(2 * half):
+        mem_cross(e).start()
     for d in range(1, n_sp):
         for copy in gate_copy(d):
             copy.start()
 
-    def mem_copy(member, c):
-        s, h = c // per_seq, (c % per_seq) * PER
-        return remote(
-            cast.at[half * member + s, pl.ds(h, PER)],
-            mem_in.at[sp, s, pl.ds(h, PER)],
-            mem_send.at[member, c],
-            mem_recv.at[sp, c],
-            member,
-            dp,
-        )
-
-    def mem_arrived(d, c):
-        s, h = c // per_seq, (c % per_seq) * PER
-        return remote(
-            cast.at[half * m + s, pl.ds(h, PER)],
-            mem_in.at[d, s, pl.ds(h, PER)],
-            mem_send.at[0, c],
-            mem_recv.at[d, c],
-            d,
-            dp,
-        )
-
-    def norm_copy(member):
-        return remote(
-            norm_ref.at[pl.ds(half * member, half)],
-            norm_in.at[sp],
-            norm_send.at[member],
-            norm_recv.at[sp],
-            member,
-            dp,
-        )
-
-    def norm_arrived(d):
-        return remote(
-            norm_ref.at[mine], norm_in.at[d], norm_send.at[0], norm_recv.at[d], d, dp
-        )
+    @pl.when(g > 0)
+    def _():
+        mem_own(0).start()
 
     for member in range(2):
 
         @pl.when(sp != member)
         def _():
             norm_copy(member).start()
-
-    @pl.loop(0, chunks)
-    def _(c):
-        for member in range(2):
-
-            @pl.when(sp != member)
-            def _():
-                mem_copy(member, c).start()
 
     @pl.loop(0, chunks)
     def _(c):
         x_copy(0, c).start()
         x_copy(1, c).start()
 
-    @pl.loop(0, direct)
+    @pl.loop(2, direct)
     def _(k):
         for j in range(1, chips):
             wy_copy(j, k).start()
@@ -294,11 +343,18 @@
         mem_in[sp] = cast[mine]
         norm_in[sp] = norm_ref[mine]
 
+    @pl.when(g > 0)
+    def _():
+        for e in range(2 * half):
+            if e > 0:
+                mem_own(e).start()
+            mem_cross_arrived(e).wait_recv()
+            mem_mate(e).start()
+
     local[0].wait()
     local[1].wait()
-    for d in range(1, n_sp):
-        for copy in gate_copy(d):
-            copy.wait_recv()
+    arrived(igr.at[pl.ds(0, n_sp - 1)], gate_recv.at[0])
+    arrived(fgr.at[pl.ds(0, n_sp - 1)], gate_recv.at[1])
 
     lane = lax.broadcasted_iota(jnp.int32, (n_groups * items, span), 1)
 
@@ -364,96 +420,79 @@
     wrow[...] = jnp.exp(mine_off - last)
     arow[...] = jnp.exp(first - last)
     srow[...] = first
-    columns = jnp.transpose(peaks[g])
-    for i in range(items):
-        pcol[i] = jnp.broadcast_to(columns[:, i : i + 1], (span, span))
-
     for copy in local[2:5]:
         copy.wait()
 
     tail_row = lax.broadcasted_iota(jnp.int32, (TAIL, width), 0)
 
     def grow(c):
-        x_copy(0, c).wait_recv()
-        x_copy(1, c).wait_recv()
         s, h = c // per_seq, (c % per_seq) * PER
-        tail = jnp.zeros((TAIL, width), f32)
+        arrived(xk.at[s, pl.ds(h, PER)], x_recv.at[0, c])
         for p in range(PER):
             key, value = xk[s, h + p], xv[s, h + p]
             w = wrow[pl.ds(c * PER + p, 1), :]
             scaled = (jnp.transpose(key.astype(f32)) * w).astype(bf16)
-            grown[c, p * width : (p + 1) * width] = jnp.dot(
-                scaled, value, preferred_element_type=f32
-            )
+            grown[c, p, :width] = jnp.dot(scaled, value, preferred_element_type=f32)
             high = w.astype(bf16).astype(f32)
             both = jnp.where(tail_row == 0, high, jnp.where(tail_row == 1, w - high, 0.0))
             norm = jnp.dot(both.astype(bf16), key, preferred_element_type=f32)
-            norm = norm[0:1] + norm[1:2]
-            tail = jnp.where(tail_row == p, norm, tail)
-        grown[c, PER * width :] = tail
-
-    def st_copy(c):
-        return remote(
-            st_out.at[c],
-            st_in.at[c],
-            st_send.at[c],
-            st_recv.at[c],
+            grown[c, p, width:] = jnp.where(tail_row == 0, norm[0:1] + norm[1:2], 0.0)
+
+    def st_copy(c, p):
+        return remote(
+            st_out.at[c, p],
+            st_in.at[c, p],
+            st_send.at[0],
+            st_recv.at[c, p],
             lax.rem(sp + 2, n_sp),
             dp,
         )
 
     def seed(c):
-        for d in range(n_sp):
-
-            @pl.when(sp != d)
-            def _():
-                mem_arrived(d, c).wait_recv()
+        per_part = chunks // (2 * half)
+
+        @pl.when(c % per_part == 0)
+        def _():
+            e = c // per_part
+            mem_cross_arrived(e).wait_recv()
+            s, h = e // 2, pl.ds((e % 2) * (heads // 2), heads // 2)
+            arrived(mem_in.at[pl.ds(2, n_sp - 2), s, h], mem_recv.at[e])
 
         @pl.when(c == 0)
         def _():
-            for d in range(n_sp):
-
-                @pl.when(sp != d)
-                def _():
-                    norm_arrived(d).wait_recv()
-
+            arrived(norm_in.at[pl.ds(0, n_sp - 1)], norm_recv.at[0])
             norm = norm_in[0].reshape(items, width)
             for d in range(1, n_sp):
                 norm = norm + norm_in[d].reshape(items, width)
             norm_out[...] = norm
 
         s, h = c // per_seq, (c % per_seq) * PER
-        tail = jnp.zeros((TAIL, width), f32)
         for p in range(PER):
             if channels % 16 == 0:
-                st_in[c, p * width : (p + 1) * width] = mem_in[:, s, h + p].reshape(width, width)
+                st_in[c, p, :width] = mem_in[:, s, h + p].reshape(width, width)
             else:
                 for d in range(n_sp):
                     whole_ref[d * channels : (d + 1) * channels] = mem_in[d, s, h + p].astype(f32)
-                st_in[c, p * width : (p + 1) * width] = whole_ref[...].astype(bf16)
-            tail = jnp.where(tail_row == p, norm_out[pl.ds(c * PER + p, 1), :], tail)
-        st_in[c, PER * width :] = tail.astype(bf16)
+                st_in[c, p, :width] = whole_ref[...].astype(bf16)
+            norm = norm_out[pl.ds(c * PER + p, 1), :]
+            st_in[c, p, width:] = jnp.where(tail_row == 0, norm, 0.0).astype(bf16)
 
     def chain(c):
         @pl.when(g == 0)
         def _():
             seed(c)
 
-        @pl.when(g > 0)
-        def _():
-            st_copy(c).wait_recv()
-
-        @pl.when(g < n_groups - 1)
-        def _():
-            tail = jnp.zeros((TAIL, width), f32)
-            for p in range(PER):
-                part = pl.ds(p * width, width)
+        for p in range(PER):
+
+            @pl.when(g > 0)
+            def _():
+                st_copy(c, p).wait_recv()
+
+            @pl.when(g < n_groups - 1)
+            def _():
                 a = arow[pl.ds(c * PER + p, 1), :]
-                st_out[c, part] = (st_in[c, part].astype(f32) * a + grown[c, part]).astype(bf16)
-                tail = jnp.where(tail_row == p, a, tail)
-            part = pl.ds(PER * width, TAIL)
-            st_out[c, part] = (st_in[c, part].astype(f32) * tail + grown[c, part]).astype(bf16)
-            st_copy(c).start()
+                st_out[c, p] = (st_in[c, p].astype(f32) * a + grown[c, p]).astype(bf16)
+                st_copy(c, p).start()
 
     def back_copy(c):
         s, h = c // per_seq, (c % per_seq) * PER
@@ -461,20 +500,8 @@
         return remote(
             back.at[s, :, lanes],
             act.at[half * m + s, :, lanes],
-            back_send.at[c],
-            back_recv.at[c],
-            mate,
-            dp,
-        )
-
-    def back_arrived(c):
-        s, h = c // per_seq, (c % per_seq) * PER
-        lanes = pl.ds(pl.multiple_of(h * width, PER * width), PER * width)
-        return remote(
-            back.at[s, :, lanes],
-            act.at[half * (1 - m) + s, :, lanes],
-            back_send.at[c],
-            back_recv.at[c],
+            back_send.at[0],
+            back_recv.at[s],
             mate,
             dp,
         )
@@ -490,9 +517,9 @@
         for p in range(PER):
             i = c * PER + p
             query, key, value = xq[s, h + p], xk[s, h + p], xv[s, h + p]
-            memory = st_in[c, p * width : (p + 1) * width]
+            memory = st_in[c, p, :width]
             norm = jnp.broadcast_to(
-                st_in[c, PER * width :].astype(f32)[p : p + 1], (width, width)
+                st_in[c, p, width:].astype(f32)[0:1], (width, width)
             ).astype(bf16)
             raw = lax.dot_general(
                 query,
@@ -517,8 +544,36 @@
             back[s, :, lanes] = jnp.where(m == 0, low, top)
         back_copy(c).start()
 
+    columns_each = weight.shape[2]
+    tile = min(512, columns_each)
+    tiles = columns_each // tile
+
+    def project(s, first, last):
+        left = jnp.concatenate([act[s], act[half + s]], axis=0)
+
+        @pl.loop(first, last)
+        def _(n):
+            j, b = n // tiles, n % tiles
+            shard = ((y + j // 2) % chips) * 2 + (core + j) % 2
+            at = pl.ds(pl.multiple_of(b * tile, tile), tile)
+            product = jnp.dot(left, weight[shard, :, at], preferred_element_type=f32).astype(bf16)
+            to = pl.ds(pl.multiple_of(shard * columns_each + b * tile, tile), tile)
+            out_ref[s, :, to] = product[:tokens]
+            out_ref[half + s, :, to] = product[tokens:]
+
+    def returned(s):
+        arrived(act.at[s], back_recv.at[s])
+
+    own_step = -(-2 * tiles // OWN_SLOTS)
     out_slot = jnp.maximum(chunks, HOP * g)
-    slots = max(chunks + max(chunks, HOP * (n_groups - 1)), 2 * SKIP)
+    slots = max(
+        chunks + max(chunks, HOP * (n_groups - 1)),
+        WHEN[-1] + 1,
+        LATE[-1] + 1,
+        WHEN_SKIP + 1,
+        WHEN_SIDE + 1,
+        WHEN_OWN + OWN_SLOTS,
+    )
 
     def pass_on(j, k):
         wy_copy(j, k).wait_recv()
@@ -530,19 +585,42 @@
         def _():
             grow(t)
 
+        for k in range(direct):
+
+            @pl.when(t == jnp.where(g == 0, LATE[k], WHEN[k]))
+            def _():
+                for j in range(1, chips):
+                    pass_on(j, k)
+                    if k < SKIP:
+                        wz_each(j, k, lambda copy: copy.start())
+                    elif k < SKIP + SIDE:
+                        wx_copy(j, k).start()
+
+        @pl.when(t == WHEN_SKIP)
+        def _():
+            for j in range(1, chips):
+                arrived(weight.at[0, pl.ds(0, SKIP * rows), :], wz_recv.at[j])
+                for k in range(SKIP):
+                    wd_copy(j, (1 - even) * SKIP + k).start()
+
+        @pl.when(t == jnp.where(g == 0, LATE[-1], WHEN_SIDE))
+        def _():
+            for j in range(1, chips):
+                arrived(weight.at[0, pl.ds(0, SIDE * rows), :], wx_recv.at[j])
+                for k in range(SIDE):
+                    wd_copy(j, 2 * SKIP + m * SIDE + k).start()
+
         c = t - HOP * g
 
         @pl.when((c >= 0) & (c < chunks))
         def _():
             chain(c)
 
-        k = (t - 1) // 2
-
-        @pl.when((t % 2 == 1) & (k < SKIP))
-        def _():
-            for j in range(1, chips):
-                pass_on(j, k)
-                wz_each(j, k, lambda copy: copy.start())
+        @pl.when(t == 1)
+        def _():
+            columns = jnp.transpose(peaks[g])
+            for i in range(items):
+                pcol[i] = jnp.broadcast_to(columns[:, i : i + 1], (span, span))
 
         o = t - out_slot
 
@@ -550,85 +628,68 @@
         def _():
             emit(o)
 
-    def pass_up_to(first, last):
-        @pl.loop(first, last)
-        def _(k):
-            for j in range(1, chips):
-                pass_on(j, k)
-
-    @pl.loop(0, SKIP)
-    def _(k):
+        @pl.when(t == WHEN_OWN)
+        def _():
+            returned(0)
+            local[9].wait()
+            own_copy().wait()
+
+        at_slot = t - WHEN_OWN
+
+        @pl.when((at_slot >= 0) & (at_slot < OWN_SLOTS))
+        def _():
+            project(0, at_slot * own_step, jnp.minimum((at_slot + 1) * own_step, 2 * tiles))
+
+    def left_all(ref, sem):
+        pltpu.make_async_copy(ref, ref, sem).wait()
+
+    def sent_early():
+        left_all(igr.at[pl.ds(0, n_sp - 1)], gate_send.at[0])
+        left_all(fgr.at[pl.ds(0, n_sp - 1)], gate_send.at[1])
+        for kind, ref in enumerate((xk, xv, xq)):
+            left_all(ref.at[:, :, pl.ds(0, tokens), :], x_send.at[kind])
+        left_all(mem_in.at[0], mem_send.at[0])
+
+        @pl.when(g > 0)
+        def _():
+            left_all(mem_in.at[0], mem_send.at[1])
+            left_all(mem_in.at[0], mem_send.at[2])
+
+        for member in range(2):
+
+            @pl.when(sp != member)
+            def _():
+                norm_copy(member).wait_send()
+
+    def sent_late():
+        left_all(back, back_send.at[0])
+
+        @pl.when(g < n_groups - 1)
+        def _():
+            left_all(st_out, st_send.at[0])
+
         for j in range(1, chips):
-            wz_copy(j, k).wait_recv()
-            wd_copy(j, (1 - even) * SKIP + k).start()
-
-    middle = (SKIP + direct) // 2
-    pass_up_to(SKIP, middle)
-
-    @pl.loop(0, chunks)
-    def _(c):
-        back_arrived(c).wait_recv()
-
-    left = act[...].reshape(seqs * tokens, heads * width)
-    columns_each = weight.shape[2]
-    tile = min(512, columns_each)
-    tiles = columns_each // tile
-
-    def project(shard):
-        @pl.loop(0, tiles)
-        def _(b):
-            at = pl.ds(pl.multiple_of(b * tile, tile), tile)
-            product = jnp.dot(left, weight[shard, :, at], preferred_element_type=f32)
-            out_ref[:, :, pl.ds(pl.multiple_of(shard * columns_each + b * tile, tile), tile)] = (
-                product.astype(bf16).reshape(seqs, tokens, tile)
-            )
-
-    local[9].wait()
-    project(dp)
-    own_copy().wait()
-    project(twin)
-    pass_up_to(middle, direct)
+            left_all(weight.at[0, pl.ds(0, direct * rows), :], wy_send.at[j])
+            left_all(weight.at[0], wd_send.at[j])
+
+            @pl.when(g > 0)
+            def _():
+                left_all(weight.at[0, pl.ds(0, SKIP * rows), :], wz_send.at[j])
+
+            @pl.when(g == n_groups - 2)
+            def _():
+                left_all(weight.at[0, pl.ds(0, SKIP * rows), :], wu_send.at[j])
+
+            left_all(weight.at[0, pl.ds(0, SIDE * rows), :], wx_send.at[j])
+
     for j in range(1, chips):
-        project(((y - j + chips) % chips) * 2 + core)
-
-        @pl.loop(0, PIECES)
-        def _(r):
-            wd_copy(j, r).wait()
-
-        project(((y - j + chips) % chips) * 2 + 1 - core)
-
-    for d in range(1, n_sp):
-        for copy in gate_copy(d):
-            copy.wait_send()
-
-    @pl.loop(0, chunks)
-    def _(c):
-        for kind in range(3):
-            x_copy(kind, c).wait_send()
-        back_copy(c).wait_send()
-
-        @pl.when(g < n_groups - 1)
-        def _():
-            st_copy(c).wait_send()
-
-    for member in range(2):
-
-        @pl.when(sp != member)
-        def _():
-            norm_copy(member).wait_send()
-
-            @pl.loop(0, chunks)
-            def _(c):
-                mem_copy(member, c).wait_send()
-
-    @pl.loop(0, direct)
-    def _(k):
-        for j in range(1, chips):
-            wy_copy(j, k).wait_send()
-
-            @pl.when(k < SKIP)
-            def _():
-                wz_each(j, k, lambda copy: copy.wait_send())
+        arrived(weight.at[0], wd_recv.at[j])
+    project(0, 2 * tiles, n_dp * tiles)
+    sent_early()
+    for s in range(1, half):
+        returned(s)
+        project(s, 0, n_dp * tiles)
+    sent_late()
 
 
 def on_device(
@@ -653,7 +714,7 @@
     groups = n_sp // 2
     chips = n_dp // 2
     chunks = items // PER
-    direct = PIECES - SKIP
+    direct = PIECES - SKIP - SIDE
     f32, bf16 = jnp.float32, jnp.bfloat16
     sizes = (n_sp, n_dp, seqs, heads, tokens, width, channels)
     operands = [
@@ -703,32 +764,35 @@
             pltpu.VMEM((items, span), f32),
             pltpu.VMEM((items, span), f32),
             pltpu.VMEM((items, span, span), f32),
-            pltpu.VMEM((chunks, PER * width + TAIL, width), f32),
-            pltpu.VMEM((chunks, PER * width + TAIL, width), bf16),
-            pltpu.VMEM((chunks, PER * width + TAIL, width), bf16),
+            pltpu.VMEM((chunks, PER, width + TAIL, width), f32),
+            pltpu.VMEM((chunks, PER, width + TAIL, width), bf16),
+            pltpu.VMEM((chunks, PER, width + TAIL, width), bf16),
             pltpu.VMEM((seqs, tokens, heads * width), bf16),
             pltpu.VMEM((half, tokens, heads * width), bf16),
             pltpu.VMEM((n_dp, mix, columns), bf16),
             dma((10,)),
-            dma((2, n_sp)),
-            dma((2, n_sp)),
-            dma((3, chunks)),
-            dma((3, chunks)),
+            dma((2,)),
+            dma((2,)),
+            dma((3,)),
             dma((2, chunks)),
-            dma((n_sp, chunks)),
+            dma((3,)),
+            dma((2 * half,)),
+            dma((2 * half,)),
             dma((2,)),
-            dma((n_sp,)),
-            dma((chunks,)),
-            dma((chunks,)),
-            dma((chunks,)),
-            dma((chunks,)),
+            dma((1,)),
+            dma((1,)),
+            dma((chunks, PER)),
+            dma((1,)),
+            dma((half,)),
+            dma((chips,)),
             dma((chips, direct)),
-            dma((chips, direct)),
-            dma((chips, SKIP)),
-            dma((chips, SKIP)),
-            dma((chips, SKIP)),
-            dma((chips, PIECES)),
-            dma((chips, PIECES)),
+            dma((chips,)),
+            dma((chips,)),
+            dma((chips,)),
+            dma((chips,)),
+            dma((chips,)),
+            dma((chips,)),
+            dma((chips,)),
             dma((1,)),
             dma((1,)),
         ],

time: 53.5 us -> 46 us (0.86)
  the two profiles are of different devices: /device:TPU:29 before, /device:TPU:1 now
where the time goes in v3:
time: 46 us; the launch traced here: 45.8 us
  Pallas kernels  44.5 us (97%)
  local copies, waits for them, and re-layouts  1.32 us (3%)
    pallas_call x1, Pallas kernels, on_device(): pl.pallas_call(lambda *refs: layer_kernel(sizes, *refs), out_shape=jax.Sh...  44.5 us
    unnamed x1, local copies, waits for them, and re-layouts  1.32 us

profile of v3, /device:TPU:1, one launch (start us, length us, event | category | flops | bytes accessed | tf_op | source)
XLA Modules:
  0.0 45.8 jit_solution(5684791511898042226)
XLA Ops:
  0.0 44.5 %layer.1 = bf16[4,64,4096]{2,1,0:T(8,128)(2,1)S(1)} custom-call(bf16[4,8,64,128]{3,2,1,0:T(8,128)(2,1)} %refs_0_.1, bf16[4,8,64,128]{3,2,1,0:T(8,128)(2,1)} %refs_1_.1, bf16[4,8,64,128]{3,2,1,0:T(8,128)(2,1)} %refs_2_.1, bf16[4,8,64]{2,1,0:T(8,128)(2,1)} %refs_3_.1, bf16[4,8,64]{2,1,0:T(8,128)(2,1)} %refs_4_.1, bf16[1024,1024]{1,0:T(8,128)(2,1)} %refs_5_.1, ...), custom_call_target="tpu_custom_call" | custom-call | tf_op jit(solution)/shard_map/layer/pallas_call | solution.py:738
  44.5 1.3 %copy.12 = bf16[4,64,4096]{2,1,0:T(8,128)(2,1)} copy(bf16[4,64,4096]{2,1,0:T(8,128)(2,1)S(1)} %layer.1) | data formatting | bytes 4194304

commit v4 on v3

--- a/solution.py
+++ b/solution.py
@@ -10,15 +10,16 @@
 PER = 2
 HOP = 3
 PIECES = 16
-SKIP = 5
+SKIP = 4
 SIDE = 2
-WHEN = (0, 1, 3, 4, 6, 8, 10, 12, 14)
-LATE = (8, 8, 8, 8, 10, 12, 15, 16, 16)
+WHEN = (0, 2, 4, 6, 8, 10)
+LATE = (8, 8, 8, 8, 9, 12)
+REST = (12, 14, 15, 15)
 WHEN_SKIP = 13
 WHEN_SIDE = 15
 OWN_SLOTS = 3
 WHEN_OWN = 14
-TAIL = 16
+TAIL = 8
 
 
 def layer_kernel(
@@ -54,6 +55,8 @@
     starts,
     off_g,
     wrow,
+    into,
+    upon,
     arow,
     srow,
     pcol,
@@ -71,7 +74,7 @@
     mem_send,
     cross_recv,
     mem_recv,
-    norm_send,
+    down_send,
     norm_recv,
     st_send,
     st_recv,
@@ -84,6 +87,8 @@
     wz_recv,
     wx_send,
     wx_recv,
+    wf_send,
+    wf_recv,
     wd_send,
     wd_recv,
     own_send,
@@ -186,9 +191,9 @@
 
     def direct_piece(k):
         side = 2 * SKIP + (1 - m) * SIDE + k - SKIP
-        return jnp.where(
-            k < SKIP, even * SKIP + k, jnp.where(k < SKIP + SIDE, side, k + SKIP + SIDE)
-        )
+        both = 2 * SKIP + m * SIDE + k - SKIP - SIDE
+        rest = jnp.where((g == 0) & (k < SKIP + 2 * SIDE), both, k + SKIP + SIDE)
+        return jnp.where(k < SKIP, even * SKIP + k, jnp.where(k < SKIP + SIDE, side, rest))
 
     def wy_copy(j, k):
         r = piece(direct_piece(k))
@@ -223,6 +228,18 @@
         def _():
             do(wz_copy(j, k, down=False))
 
+    def wf_copy(j, k):
+        shard = ((y - j + chips) % chips) * 2 + core
+        r = piece(k + SKIP + SIDE)
+        return remote(
+            weight.at[shard, r],
+            weight.at[shard, r],
+            wf_send.at[j],
+            wf_recv.at[j],
+            lax.rem(sp + n_sp - 2, n_sp),
+            dp,
+        )
+
     def wx_copy(j, k):
         shard = ((y - j + chips) % chips) * 2 + core
         r = piece(direct_piece(k))
@@ -246,81 +263,52 @@
             twin,
         )
 
-    def mem_part(e):
-        return e // 2, pl.ds((e % 2) * (heads // 2), heads // 2)
-
-    def mem_cross(e):
-        s, h = mem_part(e)
+    def mem_cross(at):
         return remote(
-            cast.at[half * (1 - m) + s, h],
-            mem_in.at[sp, s, h],
+            cast.at[pl.ds(half * (1 - m), half)],
+            mem_in.at[at],
             mem_send.at[0],
-            cross_recv.at[e],
+            cross_recv.at[0],
             mate,
             dp,
         )
 
-    def mem_cross_arrived(e):
-        s, h = mem_part(e)
+    def norm_cross(at):
         return remote(
-            cast.at[half * (1 - m) + s, h],
-            mem_in.at[mate, s, h],
-            mem_send.at[0],
-            cross_recv.at[e],
+            norm_ref.at[pl.ds(half * (1 - m), half)],
+            norm_in.at[at],
+            mem_send.at[1],
+            cross_recv.at[1],
             mate,
             dp,
         )
 
-    def mem_own(e):
-        s, h = mem_part(e)
-        return remote(
-            cast.at[half * m + s, h],
-            mem_in.at[sp, s, h],
-            mem_send.at[1],
-            mem_recv.at[e],
-            m,
-            dp,
-        )
-
-    def mem_mate(e):
-        s, h = mem_part(e)
-        return remote(
-            mem_in.at[mate, s, h],
-            mem_in.at[mate, s, h],
-            mem_send.at[2],
-            mem_recv.at[e],
-            m,
-            dp,
-        )
-
-    def norm_copy(member):
-        return remote(
-            norm_ref.at[pl.ds(half * member, half)],
-            norm_in.at[sp],
-            norm_send.at[member],
-            norm_recv.at[0],
-            member,
-            dp,
-        )
+    def mem_down(d):
+        to = lax.rem(sp + n_sp - 2 * d, n_sp)
+        return [
+            remote(cast.at[mine], mem_in.at[sp], down_send.at[0, d], mem_recv.at[g], to, dp),
+            remote(norm_ref.at[mine], norm_in.at[sp], down_send.at[1, d], norm_recv.at[g], to, dp),
+        ]
+
+    def mem_relay(d):
+        to = lax.rem(sp + n_sp - 2 * d, n_sp)
+        return [
+            remote(
+                mem_in.at[mate], mem_in.at[mate], down_send.at[2, d], mem_recv.at[g], to, dp
+            ),
+            remote(
+                norm_in.at[mate], norm_in.at[mate], down_send.at[3, d], norm_recv.at[g], to, dp
+            ),
+        ]
 
     for k in range(2):
         for j in range(1, chips):
             wy_copy(j, k).start()
-    for e in range(2 * half):
-        mem_cross(e).start()
     for d in range(1, n_sp):
         for copy in gate_copy(d):
             copy.start()
-
-    @pl.when(g > 0)
-    def _():
-        mem_own(0).start()
-
-    for member in range(2):
-
-        @pl.when(sp != member)
-        def _():
-            norm_copy(member).start()
+    mem_cross(sp).start()
+    norm_cross(sp).start()
 
     @pl.loop(0, chunks)
     def _(c):
@@ -337,19 +325,34 @@
         x_copy(2, c).start()
 
     own_copy().start()
+    for d in range(1, n_groups):
+
+        @pl.when(g >= d)
+        def _():
+            for copy in mem_down(d):
+                copy.start()
 
     @pl.when(g == 0)
     def _():
-        mem_in[sp] = cast[mine]
-        norm_in[sp] = norm_ref[mine]
-
-    @pl.when(g > 0)
-    def _():
-        for e in range(2 * half):
-            if e > 0:
-                mem_own(e).start()
-            mem_cross_arrived(e).wait_recv()
-            mem_mate(e).start()
+        st_in[...] = jnp.zeros(st_in.shape, bf16)
+
+    mem_in[sp] = cast[mine]
+    norm_in[sp] = norm_ref[mine]
+    for i in range(n_groups):
+
+        @pl.when(i < g)
+        def _():
+            mem_in[2 * i : 2 * i + 2] = jnp.zeros((2, half, heads, channels, width), bf16)
+            norm_in[2 * i : 2 * i + 2] = jnp.zeros((2, half, heads, width), f32)
+
+    mem_cross(mate).wait_recv()
+    norm_cross(mate).wait_recv()
+    for d in range(1, n_groups):
+
+        @pl.when(g >= d)
+        def _():
+            for copy in mem_relay(d):
+                copy.start()
 
     local[0].wait()
     local[1].wait()
@@ -415,6 +418,8 @@
         level = jnp.maximum(level, jnp.broadcast_to(part[:, span - 1 : span], part.shape))
     starts[n_groups] = level
     first, last = starts[g], starts[g + 1]
+    into[...] = jnp.exp(starts[0] - last)
+    upon[...] = jnp.exp(starts[0] - first)
     mine_off = offs[g]
     off_g[...] = mine_off
     wrow[...] = jnp.exp(mine_off - last)
@@ -423,6 +428,7 @@
     for copy in local[2:5]:
         copy.wait()
 
+    w_row = lax.broadcasted_iota(jnp.int32, (16, width), 0)
     tail_row = lax.broadcasted_iota(jnp.int32, (TAIL, width), 0)
 
     def grow(c):
@@ -433,10 +439,20 @@
             w = wrow[pl.ds(c * PER + p, 1), :]
             scaled = (jnp.transpose(key.astype(f32)) * w).astype(bf16)
             grown[c, p, :width] = jnp.dot(scaled, value, preferred_element_type=f32)
+            start = into[pl.ds(c * PER + p, 1), :]
+            for i in range(2):
+                whole_ref[i * channels : (i + 1) * channels] = mem_in[2 * g + i, s, h + p].astype(
+                    f32
+                )
+            rows_here = pl.ds(pl.multiple_of(g * 2 * channels, 2 * channels), 2 * channels)
+            grown[c, p, rows_here] += whole_ref[0 : 2 * channels] * start
             high = w.astype(bf16).astype(f32)
-            both = jnp.where(tail_row == 0, high, jnp.where(tail_row == 1, w - high, 0.0))
+            both = jnp.where(w_row == 0, high, jnp.where(w_row == 1, w - high, 0.0))
             norm = jnp.dot(both.astype(bf16), key, preferred_element_type=f32)
-            grown[c, p, width:] = jnp.where(tail_row == 0, norm[0:1] + norm[1:2], 0.0)
+            norm = norm[0:1] + norm[1:2]
+            for i in range(2):
+                norm = norm + norm_in[2 * g + i, s, pl.ds(h + p, 1), :] * start
+            grown[c, p, width:] = jnp.where(tail_row == 0, norm, 0.0)
 
     def st_copy(c, p):
         return remote(
@@ -448,40 +464,27 @@
             dp,
         )
 
-    def seed(c):
-        per_part = chunks // (2 * half)
-
-        @pl.when(c % per_part == 0)
-        def _():
-            e = c // per_part
-            mem_cross_arrived(e).wait_recv()
-            s, h = e // 2, pl.ds((e % 2) * (heads // 2), heads // 2)
-            arrived(mem_in.at[pl.ds(2, n_sp - 2), s, h], mem_recv.at[e])
-
-        @pl.when(c == 0)
-        def _():
-            arrived(norm_in.at[pl.ds(0, n_sp - 1)], norm_recv.at[0])
-            norm = norm_in[0].reshape(items, width)
-            for d in range(1, n_sp):
-                norm = norm + norm_in[d].reshape(items, width)
-            norm_out[...] = norm
-
-        s, h = c // per_seq, (c % per_seq) * PER
-        for p in range(PER):
-            if channels % 16 == 0:
-                st_in[c, p, :width] = mem_in[:, s, h + p].reshape(width, width)
-            else:
-                for d in range(n_sp):
-                    whole_ref[d * channels : (d + 1) * channels] = mem_in[d, s, h + p].astype(f32)
-                st_in[c, p, :width] = whole_ref[...].astype(bf16)
-            norm = norm_out[pl.ds(c * PER + p, 1), :]
-            st_in[c, p, width:] = jnp.where(tail_row == 0, norm, 0.0).astype(bf16)
+    def initial(s, h):
+        if channels % 16 == 0:
+            return mem_in[:, s, h].reshape(width, width).astype(f32)
+        for d in range(n_sp):
+            whole_ref[d * channels : (d + 1) * channels] = mem_in[d, s, h].astype(f32)
+        return whole_ref[...]
+
+    def initial_arrived():
+        for i in range(1, n_groups):
+
+            @pl.when(i > g)
+            def _():
+                arrived(mem_in.at[pl.ds(2 * i, 2)], mem_recv.at[i])
+                arrived(norm_in.at[pl.ds(2 * i, 2)], norm_recv.at[i])
+
+        norm = norm_in[0].reshape(items, width)
+        for d in range(1, n_sp):
+            norm = norm + norm_in[d].reshape(items, width)
+        norm_out[...] = norm
 
     def chain(c):
-        @pl.when(g == 0)
-        def _():
-            seed(c)
-
         for p in range(PER):
 
             @pl.when(g > 0)
@@ -517,10 +520,12 @@
         for p in range(PER):
             i = c * PER + p
             query, key, value = xq[s, h + p], xk[s, h + p], xv[s, h + p]
-            memory = st_in[c, p, :width]
-            norm = jnp.broadcast_to(
-                st_in[c, p, width:].astype(f32)[0:1], (width, width)
+            start = upon[pl.ds(i, 1), :]
+            memory = (
+                st_in[c, p, :width].astype(f32) + initial(s, h + p) * start
             ).astype(bf16)
+            norm = st_in[c, p, width:].astype(f32)[0:1] + norm_out[pl.ds(i, 1), :] * start
+            norm = jnp.broadcast_to(norm, (width, width)).astype(bf16)
             raw = lax.dot_general(
                 query,
                 jnp.concatenate([key, norm], axis=0),
@@ -548,8 +553,9 @@
     tile = min(512, columns_each)
     tiles = columns_each // tile
 
-    def project(s, first, last):
-        left = jnp.concatenate([act[s], act[half + s]], axis=0)
+    def project(which, first, last):
+        picked = [base + s for s in which for base in (0, half)]
+        left = jnp.concatenate([act[i] for i in picked], axis=0)
 
         @pl.loop(first, last)
         def _(n):
@@ -558,8 +564,12 @@
             at = pl.ds(pl.multiple_of(b * tile, tile), tile)
             product = jnp.dot(left, weight[shard, :, at], preferred_element_type=f32).astype(bf16)
             to = pl.ds(pl.multiple_of(shard * columns_each + b * tile, tile), tile)
-            out_ref[s, :, to] = product[:tokens]
-            out_ref[half + s, :, to] = product[tokens:]
+            for n_row, i in enumerate(picked):
+                out_ref[i, :, to] = product[n_row * tokens : (n_row + 1) * tokens]
+
+    def own_here():
+        local[9].wait()
+        own_copy().wait()
 
     def returned(s):
         arrived(act.at[s], back_recv.at[s])
@@ -568,8 +578,7 @@
     out_slot = jnp.maximum(chunks, HOP * g)
     slots = max(
         chunks + max(chunks, HOP * (n_groups - 1)),
-        WHEN[-1] + 1,
-        LATE[-1] + 1,
+        REST[-1] + 1,
         WHEN_SKIP + 1,
         WHEN_SIDE + 1,
         WHEN_OWN + OWN_SLOTS,
@@ -579,13 +588,40 @@
         wy_copy(j, k).wait_recv()
         wd_copy(j, direct_piece(k)).start()
 
+    def pass_rest(k):
+        for j in range(1, chips):
+            pass_on(j, k)
+            if k < SKIP + 2 * SIDE:
+
+                @pl.when(g == 1)
+                def _():
+                    wf_copy(j, k).start()
+
+    def pass_first():
+        for j in range(1, chips):
+            arrived(weight.at[0, pl.ds(0, SIDE * rows), :], wf_recv.at[j])
+            for k in range(SIDE):
+                wd_copy(j, 2 * SKIP + 2 * SIDE + k).start()
+
+    def pass_skip():
+        for j in range(1, chips):
+            arrived(weight.at[0, pl.ds(0, SKIP * rows), :], wz_recv.at[j])
+            for k in range(SKIP):
+                wd_copy(j, (1 - even) * SKIP + k).start()
+
+    def pass_side():
+        for j in range(1, chips):
+            arrived(weight.at[0, pl.ds(0, SIDE * rows), :], wx_recv.at[j])
+            for k in range(SIDE):
+                wd_copy(j, 2 * SKIP + m * SIDE + k).start()
+
     @pl.loop(0, slots)
     def _(t):
         @pl.when(t < chunks)
         def _():
             grow(t)
 
-        for k in range(direct):
+        for k in range(SKIP + SIDE):
 
             @pl.when(t == jnp.where(g == 0, LATE[k], WHEN[k]))
             def _():
@@ -593,22 +629,25 @@
                     pass_on(j, k)
                     if k < SKIP:
                         wz_each(j, k, lambda copy: copy.start())
-                    elif k < SKIP + SIDE:
-                        wx_copy(j, k).start()
-
-        @pl.when(t == WHEN_SKIP)
-        def _():
-            for j in range(1, chips):
-                arrived(weight.at[0, pl.ds(0, SKIP * rows), :], wz_recv.at[j])
-                for k in range(SKIP):
-                    wd_copy(j, (1 - even) * SKIP + k).start()
-
-        @pl.when(t == jnp.where(g == 0, LATE[-1], WHEN_SIDE))
-        def _():
-            for j in range(1, chips):
-                arrived(weight.at[0, pl.ds(0, SIDE * rows), :], wx_recv.at[j])
-                for k in range(SIDE):
-                    wd_copy(j, 2 * SKIP + m * SIDE + k).start()
+                    else:
+
+                        @pl.when(g > 0)
+                        def _():
+                            wx_copy(j, k).start()
+
+        for k in range(SKIP + SIDE, direct):
+
+            @pl.when((g == n_groups - 1) & (t == REST[k - SKIP - SIDE]))
+            def _():
+                pass_rest(k)
+
+        @pl.when((g == n_groups - 1) & (t == WHEN_SKIP))
+        def _():
+            pass_skip()
+
+        @pl.when((g == n_groups - 1) & (t == WHEN_SIDE))
+        def _():
+            pass_side()
 
         c = t - HOP * g
 
@@ -622,23 +661,26 @@
             for i in range(items):
                 pcol[i] = jnp.broadcast_to(columns[:, i : i + 1], (span, span))
 
+        @pl.when(t == out_slot)
+        def _():
+            initial_arrived()
+
         o = t - out_slot
 
         @pl.when((o >= 0) & (o < chunks))
         def _():
             emit(o)
 
-        @pl.when(t == WHEN_OWN)
+        @pl.when((g == n_groups - 1) & (t == WHEN_OWN))
         def _():
             returned(0)
-            local[9].wait()
-            own_copy().wait()
+            own_here()
 
         at_slot = t - WHEN_OWN
 
-        @pl.when((at_slot >= 0) & (at_slot < OWN_SLOTS))
-        def _():
-            project(0, at_slot * own_step, jnp.minimum((at_slot + 1) * own_step, 2 * tiles))
+        @pl.when((g == n_groups - 1) & (at_slot >= 0) & (at_slot < OWN_SLOTS))
+        def _():
+            project([0], at_slot * own_step, jnp.minimum((at_slot + 1) * own_step, 2 * tiles))
 
     def left_all(ref, sem):
         pltpu.make_async_copy(ref, ref, sem).wait()
@@ -648,18 +690,14 @@
         left_all(fgr.at[pl.ds(0, n_sp - 1)], gate_send.at[1])
         for kind, ref in enumerate((xk, xv, xq)):
             left_all(ref.at[:, :, pl.ds(0, tokens), :], x_send.at[kind])
-        left_all(mem_in.at[0], mem_send.at[0])
-
-        @pl.when(g > 0)
-        def _():
-            left_all(mem_in.at[0], mem_send.at[1])
-            left_all(mem_in.at[0], mem_send.at[2])
-
-        for member in range(2):
-
-            @pl.when(sp != member)
+        mem_cross(sp).wait_send()
+        norm_cross(sp).wait_send()
+        for d in range(1, n_groups):
+
+            @pl.when(g >= d)
             def _():
-                norm_copy(member).wait_send()
+                for copy in mem_down(d) + mem_relay(d):
+                    copy.wait_send()
 
     def sent_late():
         left_all(back, back_send.at[0])
@@ -680,15 +718,68 @@
             def _():
                 left_all(weight.at[0, pl.ds(0, SKIP * rows), :], wu_send.at[j])
 
-            left_all(weight.at[0, pl.ds(0, SIDE * rows), :], wx_send.at[j])
-
-    for j in range(1, chips):
-        arrived(weight.at[0], wd_recv.at[j])
-    project(0, 2 * tiles, n_dp * tiles)
-    sent_early()
-    for s in range(1, half):
-        returned(s)
-        project(s, 0, n_dp * tiles)
+            @pl.when(g > 0)
+            def _():
+                left_all(weight.at[0, pl.ds(0, SIDE * rows), :], wx_send.at[j])
+
+            @pl.when(g == 1)
+            def _():
+                left_all(weight.at[0, pl.ds(0, SIDE * rows), :], wf_send.at[j])
+
+    def twin_arrived():
+        for j in range(1, chips):
+            arrived(weight.at[0], wd_recv.at[j])
+
+    every = list(range(half))
+    near, far = 2 * tiles, n_dp * tiles
+
+    @pl.when(g == n_groups - 1)
+    def _():
+        twin_arrived()
+        project([0], near, far)
+        sent_early()
+        for s in every[1:]:
+            returned(s)
+        project(every[1:], 0, far)
+
+    @pl.when(g < n_groups - 1)
+    def _():
+        first = SKIP + SIDE
+        pass_rest(first)
+        pass_rest(first + 1)
+        pass_skip()
+        pass_rest(first + 2)
+
+        def ready():
+            own_here()
+            for s in every:
+                returned(s)
+
+        @pl.when(g == 0)
+        def _():
+            ready()
+            project(every, 0, near - 1)
+
+        @pl.when(g > 0)
+        def _():
+            pass_side()
+
+        for k in range(first + 3, direct):
+            pass_rest(k)
+
+        @pl.when(g == 0)
+        def _():
+            pass_first()
+
+        @pl.when(g > 0)
+        def _():
+            ready()
+
+        project(every, jnp.where(g == 0, near - 1, 0), near)
+        sent_early()
+        twin_arrived()
+        project(every, near, far)
+
     sent_late()
 
 
@@ -763,6 +854,8 @@
             pltpu.VMEM((items, span), f32),
             pltpu.VMEM((items, span), f32),
             pltpu.VMEM((items, span), f32),
+            pltpu.VMEM((items, span), f32),
+            pltpu.VMEM((items, span), f32),
             pltpu.VMEM((items, span, span), f32),
             pltpu.VMEM((chunks, PER, width + TAIL, width), f32),
             pltpu.VMEM((chunks, PER, width + TAIL, width), bf16),
@@ -775,17 +868,19 @@
             dma((2,)),
             dma((3,)),
             dma((2, chunks)),
-            dma((3,)),
-            dma((2 * half,)),
-            dma((2 * half,)),
             dma((2,)),
-            dma((1,)),
+            dma((2,)),
+            dma((groups,)),
+            dma((4, groups)),
+            dma((groups,)),
             dma((1,)),
             dma((chunks, PER)),
             dma((1,)),
             dma((half,)),
             dma((chips,)),
             dma((chips, direct)),
+            dma((chips,)),
+            dma((chips,)),
             dma((chips,)),
             dma((chips,)),
             dma((chips,)),

time: 46 us -> 42.5 us (0.924); the launches traced: 45.8 us -> 41.7 us
  Pallas kernels: 44.5 us -> 40.4 us
    pallas_call x1, Pallas kernels: 44.5 us -> 40.4 us  [on_device(): pl.pallas_call(lambda *refs: layer_kernel(sizes, *refs), out_shape=jax.Sh...]
where the time goes in v4:
time: 42.5 us; the launch traced here: 41.7 us
  Pallas kernels  40.4 us (95%)
  local copies, waits for them, and re-layouts  1.32 us (3%)
    pallas_call x1, Pallas kernels, on_device(): pl.pallas_call(lambda *refs: layer_kernel(sizes, *refs), out_shape=jax.Sh...  40.4 us
    unnamed x1, local copies, waits for them, and re-layouts  1.32 us

profile of v4, /device:TPU:1, one launch (start us, length us, event | category | flops | bytes accessed | tf_op | source)
XLA Modules:
  0.0 41.7 jit_solution(16956828060739298567)
XLA Ops:
  0.0 40.4 %layer.1 = bf16[4,64,4096]{2,1,0:T(8,128)(2,1)S(1)} custom-call(bf16[4,8,64,128]{3,2,1,0:T(8,128)(2,1)} %refs_0_.1, bf16[4,8,64,128]{3,2,1,0:T(8,128)(2,1)} %refs_1_.1, bf16[4,8,64,128]{3,2,1,0:T(8,128)(2,1)} %refs_2_.1, bf16[4,8,64]{2,1,0:T(8,128)(2,1)} %refs_3_.1, bf16[4,8,64]{2,1,0:T(8,128)(2,1)} %refs_4_.1, bf16[1024,1024]{1,0:T(8,128)(2,1)} %refs_5_.1, ...), custom_call_target="tpu_custom_call" | custom-call | tf_op jit(solution)/shard_map/layer/pallas_call | solution.py:829
  40.4 1.3 %copy.12 = bf16[4,64,4096]{2,1,0:T(8,128)(2,1)} copy(bf16[4,64,4096]{2,1,0:T(8,128)(2,1)S(1)} %layer.1) | data formatting | bytes 4194304

commit v5 on v4

--- a/solution.py
+++ b/solution.py
@@ -11,14 +11,12 @@
 HOP = 3
 PIECES = 16
 SKIP = 4
+UP = 3
 SIDE = 2
 WHEN = (0, 2, 4, 6, 8, 10)
 LATE = (8, 8, 8, 8, 9, 12)
-REST = (12, 14, 15, 15)
+REST = (12, 14)
 WHEN_SKIP = 13
-WHEN_SIDE = 15
-OWN_SLOTS = 3
-WHEN_OWN = 14
 TAIL = 8
 
 
@@ -193,7 +191,8 @@
         side = 2 * SKIP + (1 - m) * SIDE + k - SKIP
         both = 2 * SKIP + m * SIDE + k - SKIP - SIDE
         rest = jnp.where((g == 0) & (k < SKIP + 2 * SIDE), both, k + SKIP + SIDE)
-        return jnp.where(k < SKIP, even * SKIP + k, jnp.where(k < SKIP + SIDE, side, rest))
+        piece_at = jnp.where(k < SKIP, even * SKIP + k, jnp.where(k < SKIP + SIDE, side, rest))
+        return jnp.where(k < direct, piece_at, (1 - even) * SKIP + UP + k - direct)
 
     def wy_copy(j, k):
         r = piece(direct_piece(k))
@@ -224,9 +223,11 @@
         def _():
             do(wz_copy(j, k))
 
-        @pl.when(g == n_groups - 2)
-        def _():
-            do(wz_copy(j, k, down=False))
+        if k < UP:
+
+            @pl.when(g == n_groups - 2)
+            def _():
+                do(wz_copy(j, k, down=False))
 
     def wf_copy(j, k):
         shard = ((y - j + chips) % chips) * 2 + core
@@ -319,6 +320,12 @@
     def _(k):
         for j in range(1, chips):
             wy_copy(j, k).start()
+
+    @pl.when(g == n_groups - 1)
+    def _():
+        for k in range(direct, direct + SKIP - UP):
+            for j in range(1, chips):
+                wy_copy(j, k).start()
 
     @pl.loop(0, chunks)
     def _(c):
@@ -550,18 +557,17 @@
         back_copy(c).start()
 
     columns_each = weight.shape[2]
-    tile = min(512, columns_each)
+    tile = min(1024, columns_each)
     tiles = columns_each // tile
 
     def project(which, first, last):
         picked = [base + s for s in which for base in (0, half)]
         left = jnp.concatenate([act[i] for i in picked], axis=0)
 
-        @pl.loop(first, last)
-        def _(n):
+        for n in range(first, last):
             j, b = n // tiles, n % tiles
             shard = ((y + j // 2) % chips) * 2 + (core + j) % 2
-            at = pl.ds(pl.multiple_of(b * tile, tile), tile)
+            at = pl.ds(b * tile, tile)
             product = jnp.dot(left, weight[shard, :, at], preferred_element_type=f32).astype(bf16)
             to = pl.ds(pl.multiple_of(shard * columns_each + b * tile, tile), tile)
             for n_row, i in enumerate(picked):
@@ -573,15 +579,11 @@
 
     def returned(s):
         arrived(act.at[s], back_recv.at[s])
-
-    own_step = -(-2 * tiles // OWN_SLOTS)
     out_slot = jnp.maximum(chunks, HOP * g)
     slots = max(
         chunks + max(chunks, HOP * (n_groups - 1)),
         REST[-1] + 1,
         WHEN_SKIP + 1,
-        WHEN_SIDE + 1,
-        WHEN_OWN + OWN_SLOTS,
     )
 
     def pass_on(j, k):
@@ -603,10 +605,10 @@
             for k in range(SIDE):
                 wd_copy(j, 2 * SKIP + 2 * SIDE + k).start()
 
-    def pass_skip():
+    def pass_skip(count):
         for j in range(1, chips):
-            arrived(weight.at[0, pl.ds(0, SKIP * rows), :], wz_recv.at[j])
-            for k in range(SKIP):
+            arrived(weight.at[0, pl.ds(0, count * rows), :], wz_recv.at[j])
+            for k in range(count):
                 wd_copy(j, (1 - even) * SKIP + k).start()
 
     def pass_side():
@@ -635,7 +637,7 @@
                         def _():
                             wx_copy(j, k).start()
 
-        for k in range(SKIP + SIDE, direct):
+        for k in range(SKIP + SIDE, SKIP + SIDE + len(REST)):
 
             @pl.when((g == n_groups - 1) & (t == REST[k - SKIP - SIDE]))
             def _():
@@ -643,11 +645,7 @@
 
         @pl.when((g == n_groups - 1) & (t == WHEN_SKIP))
         def _():
-            pass_skip()
-
-        @pl.when((g == n_groups - 1) & (t == WHEN_SIDE))
-        def _():
-            pass_side()
+            pass_skip(UP)
 
         c = t - HOP * g
 
@@ -670,17 +668,6 @@
         @pl.when((o >= 0) & (o < chunks))
         def _():
             emit(o)
-
-        @pl.when((g == n_groups - 1) & (t == WHEN_OWN))
-        def _():
-            returned(0)
-            own_here()
-
-        at_slot = t - WHEN_OWN
-
-        @pl.when((g == n_groups - 1) & (at_slot >= 0) & (at_slot < OWN_SLOTS))
-        def _():
-            project([0], at_slot * own_step, jnp.minimum((at_slot + 1) * own_step, 2 * tiles))
 
     def left_all(ref, sem):
         pltpu.make_async_copy(ref, ref, sem).wait()
@@ -699,32 +686,35 @@
                 for copy in mem_down(d) + mem_relay(d):
                     copy.wait_send()
 
+        left_all(back, back_send.at[0])
+
+        @pl.when(g < n_groups - 1)
+        def _():
+            left_all(st_out, st_send.at[0])
+
+        for j in range(1, chips):
+
+            @pl.when(g > 0)
+            def _():
+                left_all(weight.at[0, pl.ds(0, SKIP * rows), :], wz_send.at[j])
+                left_all(weight.at[0, pl.ds(0, SIDE * rows), :], wx_send.at[j])
+
+            @pl.when(g == n_groups - 2)
+            def _():
+                left_all(weight.at[0, pl.ds(0, UP * rows), :], wu_send.at[j])
+
+            @pl.when(g == 1)
+            def _():
+                left_all(weight.at[0, pl.ds(0, SIDE * rows), :], wf_send.at[j])
+
     def sent_late():
-        left_all(back, back_send.at[0])
-
-        @pl.when(g < n_groups - 1)
-        def _():
-            left_all(st_out, st_send.at[0])
-
         for j in range(1, chips):
             left_all(weight.at[0, pl.ds(0, direct * rows), :], wy_send.at[j])
             left_all(weight.at[0], wd_send.at[j])
 
-            @pl.when(g > 0)
-            def _():
-                left_all(weight.at[0, pl.ds(0, SKIP * rows), :], wz_send.at[j])
-
-            @pl.when(g == n_groups - 2)
-            def _():
-                left_all(weight.at[0, pl.ds(0, SKIP * rows), :], wu_send.at[j])
-
-            @pl.when(g > 0)
-            def _():
-                left_all(weight.at[0, pl.ds(0, SIDE * rows), :], wx_send.at[j])
-
-            @pl.when(g == 1)
-            def _():
-                left_all(weight.at[0, pl.ds(0, SIDE * rows), :], wf_send.at[j])
+            @pl.when(g == n_groups - 1)
+            def _():
+                left_all(weight.at[0, pl.ds(0, (SKIP - UP) * rows), :], wy_send.at[j])
 
     def twin_arrived():
         for j in range(1, chips):
@@ -733,53 +723,43 @@
     every = list(range(half))
     near, far = 2 * tiles, n_dp * tiles
 
+    first = SKIP + SIDE
+
+    @pl.when(g < n_groups - 1)
+    def _():
+        for k in range(first, first + len(REST)):
+            pass_rest(k)
+        pass_skip(SKIP)
+
+    for k in range(first + len(REST), direct - 1):
+        pass_rest(k)
+
+    @pl.when(g > 0)
+    def _():
+        pass_side()
+        pass_rest(direct - 1)
+
+    sent_early()
+    own_here()
+    for s in every:
+        returned(s)
+
+    project(every, 0, max(1, near // 2))
+
+    @pl.when(g == 0)
+    def _():
+        pass_rest(direct - 1)
+        pass_first()
+
     @pl.when(g == n_groups - 1)
     def _():
-        twin_arrived()
-        project([0], near, far)
-        sent_early()
-        for s in every[1:]:
-            returned(s)
-        project(every[1:], 0, far)
-
-    @pl.when(g < n_groups - 1)
-    def _():
-        first = SKIP + SIDE
-        pass_rest(first)
-        pass_rest(first + 1)
-        pass_skip()
-        pass_rest(first + 2)
-
-        def ready():
-            own_here()
-            for s in every:
-                returned(s)
-
-        @pl.when(g == 0)
-        def _():
-            ready()
-            project(every, 0, near - 1)
-
-        @pl.when(g > 0)
-        def _():
-            pass_side()
-
-        for k in range(first + 3, direct):
-            pass_rest(k)
-
-        @pl.when(g == 0)
-        def _():
-            pass_first()
-
-        @pl.when(g > 0)
-        def _():
-            ready()
-
-        project(every, jnp.where(g == 0, near - 1, 0), near)
-        sent_early()
-        twin_arrived()
-        project(every, near, far)
-
+        for k in range(direct, direct + SKIP - UP):
+            for j in range(1, chips):
+                pass_on(j, k)
+
+    project(every, max(1, near // 2), near)
+    twin_arrived()
+    project(every, near, far)
     sent_late()
 
 
@@ -878,7 +858,7 @@
             dma((1,)),
             dma((half,)),
             dma((chips,)),
-            dma((chips, direct)),
+            dma((chips, direct + SKIP - UP)),
             dma((chips,)),
             dma((chips,)),
             dma((chips,)),

time: 42.5 us -> 41.3 us (0.972); the launches traced: 41.7 us -> 41.2 us
  Pallas kernels: 40.4 us -> 39.9 us
    pallas_call x1, Pallas kernels: 40.4 us -> 39.9 us  [on_device(): pl.pallas_call(lambda *refs: layer_kernel(sizes, *refs), out_shape=jax.Sh...]
where the time goes in v5:
time: 41.3 us; the launch traced here: 41.2 us
  Pallas kernels  39.9 us (97%)
  local copies, waits for them, and re-layouts  1.32 us (3%)
    pallas_call x1, Pallas kernels, on_device(): pl.pallas_call(lambda *refs: layer_kernel(sizes, *refs), out_shape=jax.Sh...  39.9 us
    unnamed x1, local copies, waits for them, and re-layouts  1.32 us

profile of v5, /device:TPU:1, one launch (start us, length us, event | category | flops | bytes accessed | tf_op | source)
XLA Modules:
  0.0 41.2 jit_solution(8014766181658344295)
XLA Ops:
  0.0 39.9 %layer.1 = bf16[4,64,4096]{2,1,0:T(8,128)(2,1)S(1)} custom-call(bf16[4,8,64,128]{3,2,1,0:T(8,128)(2,1)} %refs_0_.1, bf16[4,8,64,128]{3,2,1,0:T(8,128)(2,1)} %refs_1_.1, bf16[4,8,64,128]{3,2,1,0:T(8,128)(2,1)} %refs_2_.1, bf16[4,8,64]{2,1,0:T(8,128)(2,1)} %refs_3_.1, bf16[4,8,64]{2,1,0:T(8,128)(2,1)} %refs_4_.1, bf16[1024,1024]{1,0:T(8,128)(2,1)} %refs_5_.1, ...), custom_call_target="tpu_custom_call" | custom-call | tf_op jit(solution)/shard_map/layer/pallas_call | solution.py:809
  39.9 1.3 %copy.12 = bf16[4,64,4096]{2,1,0:T(8,128)(2,1)} copy(bf16[4,64,4096]{2,1,0:T(8,128)(2,1)S(1)} %layer.1) | data formatting | bytes 4194304

commit v6 on v5

--- a/solution.py
+++ b/solution.py
@@ -199,8 +199,8 @@
         return remote(
             w_hbm.at[r],
             weight.at[dp, r],
-            wy_send.at[j],
-            wy_recv.at[j, k],
+            wy_send.at[j - 1],
+            wy_recv.at[j - 1, k],
             sp,
             ((y + j) % chips) * 2 + core,
         )
@@ -212,8 +212,8 @@
         return remote(
             weight.at[shard, r],
             weight.at[shard, r],
-            (wz_send if down else wu_send).at[j],
-            wz_recv.at[j],
+            (wz_send if down else wu_send).at[j - 1],
+            wz_recv.at[j - 1],
             to,
             dp,
         )
@@ -235,8 +235,8 @@
         return remote(
             weight.at[shard, r],
             weight.at[shard, r],
-            wf_send.at[j],
-            wf_recv.at[j],
+            wf_send.at[j - 1],
+            wf_recv.at[j - 1],
             lax.rem(sp + n_sp - 2, n_sp),
             dp,
         )
@@ -247,8 +247,8 @@
         return remote(
             weight.at[shard, r],
             weight.at[shard, r],
-            wx_send.at[j],
-            wx_recv.at[j],
+            wx_send.at[j - 1],
+            wx_recv.at[j - 1],
             mate,
             dp,
         )
@@ -258,8 +258,8 @@
         return remote(
             weight.at[shard, piece(r)],
             weight.at[shard, piece(r)],
-            wd_send.at[j],
-            wd_recv.at[j],
+            wd_send.at[j - 1],
+            wd_recv.at[j - 1],
             sp,
             twin,
         )
@@ -287,18 +287,18 @@
     def mem_down(d):
         to = lax.rem(sp + n_sp - 2 * d, n_sp)
         return [
-            remote(cast.at[mine], mem_in.at[sp], down_send.at[0, d], mem_recv.at[g], to, dp),
-            remote(norm_ref.at[mine], norm_in.at[sp], down_send.at[1, d], norm_recv.at[g], to, dp),
+            remote(cast.at[mine], mem_in.at[sp], down_send.at[0, d - 1], mem_recv.at[g], to, dp),
+            remote(norm_ref.at[mine], norm_in.at[sp], down_send.at[1, d - 1], norm_recv.at[g], to, dp),
         ]
 
     def mem_relay(d):
         to = lax.rem(sp + n_sp - 2 * d, n_sp)
         return [
             remote(
-                mem_in.at[mate], mem_in.at[mate], down_send.at[2, d], mem_recv.at[g], to, dp
+                mem_in.at[mate], mem_in.at[mate], down_send.at[2, d - 1], mem_recv.at[g], to, dp
             ),
             remote(
-                norm_in.at[mate], norm_in.at[mate], down_send.at[3, d], norm_recv.at[g], to, dp
+                norm_in.at[mate], norm_in.at[mate], down_send.at[3, d - 1], norm_recv.at[g], to, dp
             ),
         ]
 
@@ -601,19 +601,19 @@
 
     def pass_first():
         for j in range(1, chips):
-            arrived(weight.at[0, pl.ds(0, SIDE * rows), :], wf_recv.at[j])
+            arrived(weight.at[0, pl.ds(0, SIDE * rows), :], wf_recv.at[j - 1])
             for k in range(SIDE):
                 wd_copy(j, 2 * SKIP + 2 * SIDE + k).start()
 
     def pass_skip(count):
         for j in range(1, chips):
-            arrived(weight.at[0, pl.ds(0, count * rows), :], wz_recv.at[j])
+            arrived(weight.at[0, pl.ds(0, count * rows), :], wz_recv.at[j - 1])
             for k in range(count):
                 wd_copy(j, (1 - even) * SKIP + k).start()
 
     def pass_side():
         for j in range(1, chips):
-            arrived(weight.at[0, pl.ds(0, SIDE * rows), :], wx_recv.at[j])
+            arrived(weight.at[0, pl.ds(0, SIDE * rows), :], wx_recv.at[j - 1])
             for k in range(SIDE):
                 wd_copy(j, 2 * SKIP + m * SIDE + k).start()
 
@@ -696,29 +696,29 @@
 
             @pl.when(g > 0)
             def _():
-                left_all(weight.at[0, pl.ds(0, SKIP * rows), :], wz_send.at[j])
-                left_all(weight.at[0, pl.ds(0, SIDE * rows), :], wx_send.at[j])
+                left_all(weight.at[0, pl.ds(0, SKIP * rows), :], wz_send.at[j - 1])
+                left_all(weight.at[0, pl.ds(0, SIDE * rows), :], wx_send.at[j - 1])
 
             @pl.when(g == n_groups - 2)
             def _():
-                left_all(weight.at[0, pl.ds(0, UP * rows), :], wu_send.at[j])
+                left_all(weight.at[0, pl.ds(0, UP * rows), :], wu_send.at[j - 1])
 
             @pl.when(g == 1)
             def _():
-                left_all(weight.at[0, pl.ds(0, SIDE * rows), :], wf_send.at[j])
+                left_all(weight.at[0, pl.ds(0, SIDE * rows), :], wf_send.at[j - 1])
 
     def sent_late():
         for j in range(1, chips):
-            left_all(weight.at[0, pl.ds(0, direct * rows), :], wy_send.at[j])
-            left_all(weight.at[0], wd_send.at[j])
+            left_all(weight.at[0, pl.ds(0, direct * rows), :], wy_send.at[j - 1])
+            left_all(weight.at[0], wd_send.at[j - 1])
 
             @pl.when(g == n_groups - 1)
             def _():
-                left_all(weight.at[0, pl.ds(0, (SKIP - UP) * rows), :], wy_send.at[j])
+                left_all(weight.at[0, pl.ds(0, (SKIP - UP) * rows), :], wy_send.at[j - 1])
 
     def twin_arrived():
         for j in range(1, chips):
-            arrived(weight.at[0], wd_recv.at[j])
+            arrived(weight.at[0], wd_recv.at[j - 1])
 
     every = list(range(half))
     near, far = 2 * tiles, n_dp * tiles
@@ -851,23 +851,23 @@
             dma((2,)),
             dma((2,)),
             dma((groups,)),
-            dma((4, groups)),
+            dma((4, groups - 1)),
             dma((groups,)),
             dma((1,)),
             dma((chunks, PER)),
             dma((1,)),
             dma((half,)),
-            dma((chips,)),
-            dma((chips, direct + SKIP - UP)),
-            dma((chips,)),
-            dma((chips,)),
-            dma((chips,)),
-            dma((chips,)),
-            dma((chips,)),
-            dma((chips,)),
-            dma((chips,)),
-            dma((chips,)),
-            dma((chips,)),
+            dma((chips - 1,)),
+            dma((chips - 1, direct + SKIP - UP)),
+            dma((chips - 1,)),
+            dma((chips - 1,)),
+            dma((chips - 1,)),
+            dma((chips - 1,)),
+            dma((chips - 1,)),
+            dma((chips - 1,)),
+            dma((chips - 1,)),
+            dma((chips - 1,)),
+            dma((chips - 1,)),
             dma((1,)),
             dma((1,)),
         ],

time: 41.3 us -> 41.1 us (level)
  no operation moved by 1% of the time
where the time goes in v6:
time: 41.1 us; the launch traced here: 41 us
  Pallas kernels  39.6 us (96%)
  local copies, waits for them, and re-layouts  1.32 us (3%)
    pallas_call x1, Pallas kernels, on_device(): pl.pallas_call(lambda *refs: layer_kernel(sizes, *refs), out_shape=jax.Sh...  39.6 us
    unnamed x1, local copies, waits for them, and re-layouts  1.32 us

profile of v6, /device:TPU:1, one launch (start us, length us, event | category | flops | bytes accessed | tf_op | source)
XLA Modules:
  0.0 41.0 jit_solution(10904022077597381254)
XLA Ops:
  0.0 39.6 %layer.1 = bf16[4,64,4096]{2,1,0:T(8,128)(2,1)S(1)} custom-call(bf16[4,8,64,128]{3,2,1,0:T(8,128)(2,1)} %refs_0_.1, bf16[4,8,64,128]{3,2,1,0:T(8,128)(2,1)} %refs_1_.1, bf16[4,8,64,128]{3,2,1,0:T(8,128)(2,1)} %refs_2_.1, bf16[4,8,64]{2,1,0:T(8,128)(2,1)} %refs_3_.1, bf16[4,8,64]{2,1,0:T(8,128)(2,1)} %refs_4_.1, bf16[1024,1024]{1,0:T(8,128)(2,1)} %refs_5_.1, ...), custom_call_target="tpu_custom_call" | custom-call | tf_op jit(solution)/shard_map/layer/pallas_call | solution.py:809
  39.6 1.3 %copy.12 = bf16[4,64,4096]{2,1,0:T(8,128)(2,1)} copy(bf16[4,64,4096]{2,1,0:T(8,128)(2,1)S(1)} %layer.1) | data formatting | bytes 4194304
